TPU v7x, 128 devices: a whole 4x4x4 slice. The times are simulated.
128 devices in a mesh: sp: 16 (over z, y), tp: 8 (over x, core).
Axes of the slice: x: 4, y: 4, z: 4, core: 2. Of those that a mesh axis runs over, the one named last changes fastest.
Arguments:
- residual: bfloat16 [10240, 2048], P('sp', 'tp'), may hold values from -4 to 4
- query_wide: bfloat16 [10240, 1536], P('sp', 'tp'), may hold values from -500 to 500
- query_narrow: bfloat16 [10240, 1024], P('sp', 'tp'), may hold values from -500 to 500
- latent: bfloat16 [10240, 512], P('sp'), may hold values from -6 to 6
- rope_key: bfloat16 [10240, 64], P('sp'), may hold values from -6 to 6
- latent_gain: float32 [512], replicated, may hold values from 0.1 to 1.9
- expand_wide: bfloat16 [512, 2048], P(None, 'tp'), may hold values from -0.25 to 0.25
- expand_narrow: bfloat16 [512, 1024], P(None, 'tp'), may hold values from -0.25 to 0.25
- out_wide: bfloat16 [1024, 2048], P('tp'), may hold values from -0.1875 to 0.1875
- out_narrow: bfloat16 [512, 2048], P('tp'), may hold values from -0.25 to 0.25
- norm_gain: float32 [2048], P('tp'), may hold values from 0.1 to 1.9
- up_gate: bfloat16 [2048, 5632], P('sp', 'tp'), may hold values from -0.125 to 0.125
- up_value: bfloat16 [2048, 5632], P('sp', 'tp'), may hold values from -0.125 to 0.125
- down_weight: bfloat16 [2048, 5632], P('sp', 'tp'), may hold values from -0.078125 to 0.078125
- conv_taps: float32 [3, 2, 5632], P(None, None, 'tp'), may hold values from -3 to 3
Outputs:
- output: bfloat16 [10240, 2048], P('sp', 'tp')
All inputs are finite; a program needn't handle non-finite values.
Results may differ from a plain program's by a relative error of at most 0.025.
Values may be sent and summed in bfloat16 or wider, within the bound.
A program may use at most 192 MiB of HBM per device.

v0:
```python
import jax
import jax.numpy as jnp
from jax import lax
from jax.sharding import Mesh
from jax.sharding import PartitionSpec as P

D = 2048
ROPE = 64
NOPE_W = 128
VAL_W = 128
NOPE_N = 64
VAL_N = 64
SP = ("sp_0", "sp_1")


theta = 10000.0
epsilon = 1e-06


def sent_together(arrays, axis, dim, along):
    ends, at = ([], 0)
    for a in arrays[:-1]:
        at += a.shape[along]
        ends.append(at)
    both = jnp.concatenate(arrays, axis=along)
    return tuple(jnp.split(lax.all_gather(both, axis, axis=dim, tiled=True), ends, axis=along))


def in_blocks(shard, dim, count):
    shape = shard.shape
    blocks = shard.reshape(*shape[:dim], count, shape[dim] // count, *shape[dim + 1 :])
    return jnp.moveaxis(blocks, dim, 0)


def sum_at_owner(shard, axis, dim):
    count = lax.axis_size(axis)
    blocks = lax.all_to_all(in_blocks(shard, dim, count), axis, 0, 0, tiled=True)
    return jnp.sum(blocks.astype(jnp.float32), axis=0)


def from_everyone(shard, axis):
    count = lax.axis_size(axis)
    return lax.all_to_all(
        jnp.broadcast_to(shard[None], (count, *shard.shape)), axis, 0, 0, tiled=True
    )


def over_copies(shard, axis):
    return from_everyone(shard, axis).sum(axis=0)


def joined_along(blocks, dim):
    shape = list(blocks.shape[1:])
    shape[dim] *= blocks.shape[0]
    return jnp.moveaxis(blocks, 0, dim).reshape(shape)


def collect(shard, axis, dim):
    blocks = from_everyone(shard, axis)
    return joined_along(blocks, dim)


def gathered_by_axis(shard, axes, dim):
    if not axes:
        return shard
    nearer = lax.all_gather(shard, axes[-1], axis=dim, tiled=True)
    return gathered_by_axis(nearer, axes[:-1], dim)


def padded(block, sides, width):
    for axis, dim in sides:
        count = lax.axis_size(axis)
        forward = [(i, i + 1) for i in range(count - 1)]
        backward = [(target, source) for source, target in forward]
        low = lax.ppermute(
            lax.slice_in_dim(block, block.shape[dim] - width, None, axis=dim), axis, forward
        )
        high = lax.ppermute(lax.slice_in_dim(block, 0, width, axis=dim), axis, backward)
        block = jnp.concatenate([low, block, high], axis=dim)
    return block


def rotate(values, positions):
    half_dim = values.shape[-1] // 2
    inverse = jnp.power(
        jnp.float32(theta), -2.0 * jnp.arange(half_dim, dtype=jnp.float32) / values.shape[-1]
    )
    angles = positions[:, None] * inverse[None, :]
    new_shape = (angles.shape[0],) + (1,) * (values.ndim - 2) + (half_dim,)
    cosine = jnp.cos(angles).reshape(new_shape)
    sine_part = jnp.sin(angles).reshape(new_shape)
    floats = values.astype(jnp.float32)
    lower_half = floats[..., :half_dim]
    upper_half = floats[..., half_dim:]
    turned = jnp.concatenate(
        [
            lower_half * cosine - upper_half * sine_part,
            lower_half * sine_part + upper_half * cosine,
        ],
        axis=-1,
    )
    return turned.astype(jnp.bfloat16)


def turn_query(queries, head_count, nope_dim, positions):
    shaped = queries.reshape(queries.shape[0], head_count, nope_dim + ROPE)
    return jnp.concatenate(
        [shaped[..., :nope_dim], rotate(shaped[..., nope_dim:], positions)], axis=-1
    )


def start_state(head_count, tok_rows, value_dim):
    return (
        jnp.full((head_count, tok_rows), -1e30, jnp.float32),
        jnp.zeros((head_count, tok_rows), jnp.float32),
        jnp.zeros((head_count, tok_rows, value_dim), jnp.float32),
    )


def attend_piece(carry_state, query_turned, nope_dim, kv_piece, rope_piece, factor):
    scores = jnp.einsum(
        "qhd,khd->hqk",
        query_turned[..., :nope_dim],
        kv_piece[..., :nope_dim],
        preferred_element_type=jnp.float32,
    )
    scores = (
        scores
        + jnp.einsum(
            "qhd,kd->hqk",
            query_turned[..., nope_dim:],
            rope_piece,
            preferred_element_type=jnp.float32,
        )
    ) * factor
    row_max, row_total, weighted = carry_state
    new_max = jnp.maximum(row_max, jnp.max(scores, axis=-1))
    weights = jnp.exp(scores - new_max[:, :, None])
    row_total = jnp.sum(weights, axis=-1)
    weighted = jnp.einsum(
        "hqk,khd->hqd",
        weights.astype(jnp.bfloat16),
        kv_piece[..., nope_dim:],
        preferred_element_type=jnp.float32,
    )
    return (new_max, row_total, weighted)


def finish(carry_state):
    row_max, row_total, weighted = carry_state
    normalized = weighted / row_total[:, :, None]
    return (
        jnp.transpose(normalized, (1, 0, 2)).reshape(normalized.shape[1], -1).astype(jnp.bfloat16)
    )


def per_device(
    residual,
    query_wide,
    query_narrow,
    latent,
    rope_key,
    latent_gain,
    expand_wide,
    expand_narrow,
    out_wide,
    out_narrow,
    norm_gain,
    up_gate,
    up_value,
    down_weight,
    conv_taps,
):
    tok_rows = residual.shape[0]
    offset = lax.axis_index(SP) * tok_rows
    positions = (offset + lax.iota(jnp.int32, tok_rows)).astype(jnp.float32)
    latent_float = latent.astype(jnp.float32)
    normed_latent = (
        latent_float
        * lax.rsqrt(jnp.mean(latent_float * latent_float, axis=-1, keepdims=True) + epsilon)
        * latent_gain
    ).astype(jnp.bfloat16)
    rope_turned = rotate(rope_key, positions)
    wide_heads = query_wide.shape[1] // (NOPE_W + ROPE)
    narrow_heads = query_narrow.shape[1] // (NOPE_N + ROPE)
    query_w = turn_query(query_wide, wide_heads, NOPE_W, positions)
    query_n = turn_query(query_narrow, narrow_heads, NOPE_N, positions)
    carry_init = (
        start_state(wide_heads, tok_rows, VAL_W),
        start_state(narrow_heads, tok_rows, VAL_N),
    )
    own_wide = jnp.dot(normed_latent, expand_wide, preferred_element_type=jnp.float32).astype(
        jnp.bfloat16
    )
    own_narrow = jnp.dot(normed_latent, expand_narrow, preferred_element_type=jnp.float32).astype(
        jnp.bfloat16
    )
    pieces = sent_together((own_wide, own_narrow, rope_turned), SP, 0, 1)
    kv_wide = pieces[0]
    kv_narrow = pieces[1]
    rope_piece = pieces[2]
    piece_rows = rope_piece.shape[0]
    kv_wide = kv_wide.reshape(piece_rows, wide_heads, NOPE_W + VAL_W)
    kv_narrow = kv_narrow.reshape(piece_rows, narrow_heads, NOPE_N + VAL_N)
    wide_state = attend_piece(
        carry_init[0], query_w, NOPE_W, kv_wide, rope_piece, (NOPE_W + ROPE) ** (-0.5)
    )
    narrow_state = attend_piece(
        carry_init[1], query_n, NOPE_N, kv_narrow, rope_piece, (NOPE_N + ROPE) ** (-0.5)
    )
    heads_wide = finish(wide_state)
    heads_narrow = finish(narrow_state)
    head_terms = jnp.dot(heads_wide, out_wide, preferred_element_type=jnp.float32)
    head_terms = head_terms + jnp.dot(heads_narrow, out_narrow, preferred_element_type=jnp.float32)
    head_shares = sum_at_owner(head_terms.astype(jnp.bfloat16), "tp", 1)
    attended = (residual.astype(jnp.float32) + head_shares).astype(jnp.bfloat16)
    attended_float = attended.astype(jnp.float32)
    squares = over_copies(jnp.sum(attended_float * attended_float, axis=-1), "tp")
    factor_rows = lax.rsqrt(squares / D + epsilon)
    normed_own = (attended_float * factor_rows[:, None] * norm_gain).astype(jnp.bfloat16)
    normed_full = collect(normed_own, "tp", 1)
    pieces = sent_together((up_gate, up_value), SP, 0, 1)
    gate_float = jnp.dot(normed_full, pieces[0], preferred_element_type=jnp.float32)
    value_float = jnp.dot(normed_full, pieces[1], preferred_element_type=jnp.float32)
    down_full = gathered_by_axis(down_weight, SP, 0)
    gate_width = up_gate.shape[1]
    both_up = jnp.concatenate(
        [gate_float.astype(jnp.bfloat16), value_float.astype(jnp.bfloat16)], axis=1
    )
    extended = padded(both_up, ((SP, 0),), 1).astype(jnp.float32)
    tap_rows = conv_taps.reshape(3, 2 * gate_width)
    smoothed = (
        tap_rows[0] * extended[:-2] + tap_rows[1] * extended[1:-1] + tap_rows[2] * extended[2:]
    )
    hidden = (jax.nn.silu(smoothed[:, :gate_width]) * smoothed[:, gate_width:]).astype(jnp.bfloat16)
    unit_terms = lax.dot_general(
        hidden, down_full, (((1,), (1,)), ((), ())), preferred_element_type=jnp.float32
    )
    unit_shares = sum_at_owner(unit_terms.astype(jnp.bfloat16), "tp", 1)
    return (attended_float + unit_shares).astype(jnp.bfloat16)


def solution(mesh):
    split = Mesh(mesh.devices.reshape(4, 4, mesh.shape["tp"]), ("sp_0", "sp_1", "tp"))
    in_specs = (
        P(SP, "tp"),
        P(SP, "tp"),
        P(SP, "tp"),
        P(SP, None),
        P(SP, None),
        P(),
        P(None, "tp"),
        P(None, "tp"),
        P("tp", None),
        P("tp", None),
        P("tp"),
        P(SP, "tp"),
        P(SP, "tp"),
        P(SP, "tp"),
        P(None, None, "tp"),
    )
    out_specs = P(SP, "tp")
    return jax.shard_map(
        per_device, mesh=split, in_specs=in_specs, out_specs=out_specs, check_vma=False
    )
```

profile of v0, /device:TPU:1, one launch (start us, length us, event | category | flops | bytes accessed | tf_op | source)
XLA Modules:
  0.0 370.8 jit_solution(8747017201565066184)
XLA Ops:
  6.5 0.0 all-gather.4.cloned.1.call-start
  6.6 1.0 convert_element_type.93
  7.6 0.0 copy-start.5
  7.6 1.3 fusion.28
  9.0 1.7 convolution_convert_fusion.1
  10.6 1.6 convolution_convert_fusion.2
  12.2 0.4 fusion.91
  12.6 0.9 pad_maximum_fusion
  13.5 0.0 all-gather.4.cloned.1.call-update
  13.5 0.0 all-gather.6.cloned.1.call-start
  13.6 0.8 pad_maximum_fusion.3
  14.3 0.0 all-gather.6.cloned.1.call-update
  14.4 0.2 copy.27
  14.6 0.0 copy-done.5
  14.6 0.1 slice_convert_fusion
  14.7 2.2 fusion.85
  16.9 74.5 %all-gather.4.cloned.1.call-done = bf16[10240,448]{0,1:T(8,128)(2,1)} async-done(((bf16[640,448]{0,1:T(8,128)(2,1)}), bf16[10240,448]{0,1:T(8,128)(2,1)}) %all-gather.4.cloned.1.call-update) | async-done | bytes 9175056 | tf_op jit(solution)/shard_map/all_gather | solution.py:26
  91.4 2.1 slice_bitcast_fusion.1
  93.5 0.0 slice-start.1
  93.5 0.0 slice-start.2
  93.5 12.0 %fusion.31 = f32[10240,640]{1,0:T(8,128)} fusion(bf16[10240,1,128]{0,2,1:T(8,128)(2,1)S(1)} %slice_bitcast_fusion.1, bf16[640,1,128]{2,0,1:T(8,128)(2,1)} %bitcast.114), kind=kOutput, calls=%fused_computation.47 | convolution fusion | flops 838860800 | bytes 27688960 | tf_op jit(solution)/shard_map/qhd,khd->hqk/dot_general | solution.py:121
  105.6 0.5 slice_bitcast_fusion
  106.1 10.6 %fusion.20 = f32[10240,640]{1,0:T(8,128)} fusion(bf16[10240,1,256]{0,2,1:T(8,128)(2,1)S(1)} %slice_bitcast_fusion, bf16[640,1,192]{2,0,1:T(8,128)(2,1)S(1)} %bitcast.113), kind=kOutput, calls=%fused_computation.35 | convolution fusion | flops 1677721600 | bytes 28999680 | tf_op jit(solution)/shard_map/qhd,khd->hqk/dot_general | solution.py:121
  116.7 18.2 %fusion.99 = (f32[640]{0:T(1024)S(1)}, f32[1,640,10240]{1,2,0:T(8,128)}) fusion(bf16[640,32]{1,0:T(8,128)(2,1)} %get-tuple-element.18, bf16[640,32]{1,0:T(8,128)(2,1)} %get-tuple-element.19, bf16[10240,448]{0,1:T(8,128)(2,1)} %all-gather.4.cloned.1.call-done, f32[10240,640]{1,0:T(8,128)} %fusion.31), kind=kOutput, calls=%fused_computation.125 | convolution fusion | flops 858684800 | bytes 54069760 | tf_op jit(solution)/shard_map/qhd,kd->hqk/dot_general | solution.py:129
  135.0 0.0 copy-done.4
  135.0 19.0 %fusion.100 = (f32[640]{0:T(1024)S(1)}, f32[1,640,10240]{1,2,0:T(8,128)}) fusion(bf16[640,32]{1,0:T(8,128)(2,1)S(1)} %copy-done.4, bf16[640,32]{1,0:T(8,128)(2,1)S(1)} %copy-done.3, bf16[10240,448]{0,1:T(8,128)(2,1)} %all-gather.4.cloned.1.call-done, f32[10240,640]{1,0:T(8,128)} %fusion.20), kind=kOutput, calls=%fused_computation.126 | convolution fusion | flops 858684800 | bytes 53824000 | tf_op jit(solution)/shard_map/qhd,kd->hqk/dot_general | solution.py:129
  153.9 10.7 %fusion.4 = f32[640]{0:T(1024)S(1)} fusion(f32[1,640,10240]{1,2,0:T(8,128)} %get-tuple-element.21, f32[640]{0:T(1024)S(1)} %broadcast_maximum_fusion), kind=kLoop, calls=%fused_computation.8 | loop fusion | flops 13106560 | bytes 26219520 | tf_op jit(solution)/shard_map/reduce_sum | solution.py:139
  164.6 5.3 %copy-done.1 = f32[1,640,10240]{1,2,0:T(8,128)S(1)} copy-done((f32[1,640,10240]{1,2,0:T(8,128)S(1)}, f32[1,640,10240]{1,2,0:T(8,128)}, u32[]{:S(2)}) %copy-start.1) | copy-done | bytes 26214424
  169.9 4.1 %fusion.2 = f32[640]{0:T(1024)S(1)} fusion(f32[1,640,10240]{1,2,0:T(8,128)S(1)} %copy-done.1, f32[640]{0:T(1024)S(1)} %broadcast_maximum_fusion.1), kind=kLoop, calls=%fused_computation.6 | loop fusion | flops 13106560 | bytes 26219520 | tf_op jit(solution)/shard_map/reduce_sum | solution.py:139
  174.1 15.7 %fusion.41 = f32[640,2048]{1,0:T(8,128)} fusion(bf16[64,2048]{1,0:T(8,128)(2,1)S(1)} %copy-done.7, f32[1,640,10240]{1,2,0:T(8,128)} %get-tuple-element.21, f32[640]{0:T(1024)S(1)} %broadcast_maximum_fusion, bf16[10240,1,128]{0,2,1:T(8,128)(2,1)S(1)} %slice_bitcast_fusion.1, f32[640]{0:T(1024)S(1)} %fusion.4), kind=kOutput, calls=%fused_computation.55 | convolution fusion | flops 1019822080 | bytes 33038336 | tf_op jit(solution)/shard_map/dot_general | solution.py:214
  189.8 16.3 %add_convert_fusion = bf16[640,2048]{1,0:T(8,128)(2,1)S(1)} fusion(f32[640,2048]{1,0:T(8,128)} %fusion.41, bf16[128,2048]{1,0:T(8,128)(2,1)S(1)} %copy-done, bf16[10240,1,256]{0,2,1:T(8,128)(2,1)} %copy-done.2, f32[1,640,10240]{1,2,0:T(8,128)} %get-tuple-element.23, f32[640]{0:T(1024)S(1)} %broadcast_maximum_fusion.1, f32[640]{0:T(1024)S(1)} %fusion.2), kind=kOutput, calls=%fused_computation.19 | convolution fusion | flops 2029158400 | bytes 37229568 | tf_op jit(solution)/shard_map/dot_general | solution.py:213
  206.1 0.2 copy.38
  206.3 0.0 copy-start.6
  206.3 36.8 %all_to_all.21 = bf16[8,640,256]{2,1,0:T(8,128)(2,1)S(1)} all-to-all(bf16[8,640,256]{2,1,0:T(8,128)(2,1)S(1)} %bitcast.109), channel_id=1, replica_groups=mesh['sp_0'=4,'sp_1'=4,'tp'=8] {'tp'}, dimensions={0} | all-to-all | bytes 5242880 | tf_op jit(solution)/shard_map/all_to_all | solution.py:37
  243.1 0.4 convert_reduce_fusion.1
  243.5 0.2 fusion.53
  243.7 8.1 %all_to_all.22 = f32[8,1,640]{2,1,0:T(1,128)S(1)} all-to-all(f32[8,1,640]{2,1,0:T(1,128)S(1)} %broadcast_in_dim.4), channel_id=1, replica_groups=mesh['sp_0'=4,'sp_1'=4,'tp'=8] {'tp'}, dimensions={0} | all-to-all | bytes 40960 | tf_op jit(solution)/shard_map/all_to_all | solution.py:43
  251.8 0.2 fusion.55
  252.0 0.2 copy.30
  252.2 0.0 copy-start.9
  252.2 1.7 broadcast_in_dim.5
  254.0 5.0 %all-to-all-start.2 = ((bf16[8,640,256]{1,2,0:T(8,128)(2,1)}), bf16[8,640,256]{1,2,0:T(8,128)(2,1)}, u32[]{:S(2)}, u32[]{:S(2)}) async-start(bf16[8,640,256]{1,2,0:T(8,128)(2,1)} %broadcast_in_dim.5), calls=%async_computation.2 | async-start | bytes 5242880 | tf_op jit(solution)/shard_map/all_to_all | solution.py:43
  258.9 16.0 %all_gather.14 = bf16[512,704]{0,1:T(8,128)(2,1)} all-gather(bf16[128,704]{0,1:T(8,128)(2,1)S(1)} %copy-done.9), channel_id=1, replica_groups=mesh['sp_0'=4,'sp_1'=4,'tp'=8] {'sp_1'}, dimensions={0}, use_global_device_ids=true | all-gather | bytes 901120 | tf_op jit(solution)/shard_map/all_gather | solution.py:66
  275.0 0.0 all-gather.8.cloned.1.call-update
  275.0 0.0 all-gather.6.cloned.1.call-done
  275.0 15.9 %all-to-all-done.2 = bf16[8,640,256]{1,2,0:T(8,128)(2,1)} async-done(((bf16[8,640,256]{1,2,0:T(8,128)(2,1)}), bf16[8,640,256]{1,2,0:T(8,128)(2,1)}, u32[]{:S(2)}, u32[]{:S(2)}) %all-to-all-start.2) | async-done | bytes 2621472 | tf_op jit(solution)/shard_map/all_to_all | solution.py:43
  290.9 5.2 %fusion.22 = bf16[640,704]{0,1:T(8,128)(2,1)S(1)} fusion(bf16[640,2048]{0,1:T(8,128)(2,1)} %bitcast.26, bf16[2048,1408]{0,1:T(8,128)(2,1)} %all-gather.6.cloned.1.call-done), kind=kOutput, calls=%fused_computation.41 | convolution fusion | flops 1845944320 | bytes 6406144 | tf_op jit(solution)/shard_map/dot_general | solution.py:223
  296.1 0.0 copy-start.12
  296.1 4.2 %fusion.25 = bf16[640,704]{0,1:T(8,128)(2,1)S(1)} fusion(bf16[640,2048]{0,1:T(8,128)(2,1)} %bitcast.26, bf16[2048,1408]{0,1:T(8,128)(2,1)S(1)} %copy-done.14), kind=kOutput, calls=%fused_computation.42 | convolution fusion | flops 1845944320 | bytes 6406144 | tf_op jit(solution)/shard_map/dot_general | solution.py:224
  300.3 0.2 pad_maximum_fusion.2
  300.5 3.9 %collective-permute-start = (bf16[1,1408]{0,1:T(8,128)(2,1)S(1)}, bf16[1,1408]{0,1:T(8,128)(2,1)}, u32[]{:S(2)}, u32[]{:S(2)}) collective-permute-start(bf16[1,1408]{0,1:T(8,128)(2,1)S(1)} %get-tuple-element.7), channel_id=1, source_target_pairs={{0,8},{8,16},{16,24},{24,32},{32,40},{40,48},{48,56},{56,64},{64,7... | collective-permute-start | bytes 8456 | tf_op jit(solution)/shard_map/ppermute | solution.py:75
  304.4 1.3 collective-permute-start.1
  305.7 0.1 mul.206
  305.7 0.1 mul.214
  305.8 0.1 mul.217
  305.9 4.5 %collective-permute-done = bf16[1,1408]{0,1:T(8,128)(2,1)} collective-permute-done((bf16[1,1408]{0,1:T(8,128)(2,1)S(1)}, bf16[1,1408]{0,1:T(8,128)(2,1)}, u32[]{:S(2)}, u32[]{:S(2)}) %collective-permute-start) | collective-permute-done | bytes 2848 | tf_op jit(solution)/shard_map/ppermute | solution.py:75
  310.4 4.7 %collective-permute-done.1 = bf16[1,1408]{0,1:T(8,128)(2,1)} collective-permute-done((bf16[1,1408]{0,1:T(8,128)(2,1)S(1)}, bf16[1,1408]{0,1:T(8,128)(2,1)}, u32[]{:S(2)}, u32[]{:S(2)}) %collective-permute-start.1) | collective-permute-done | bytes 2848 | tf_op jit(solution)/shard_map/ppermute | solution.py:78
  315.1 2.2 maximum_convert_fusion
  317.3 4.1 %fusion.14 = f32[640,1408]{0,1:T(8,128)} fusion(f32[642,1408]{0,1:T(8,128)S(1)} %maximum_convert_fusion, f32[1408]{0:T(1024)S(1)} %mul.217, f32[1408]{0:T(1024)S(1)} %mul.214, f32[1408]{0:T(1024)S(1)} %mul.206), kind=kLoop, calls=%fused_computation.21 | loop fusion | flops 4505600 | bytes 14434816 | tf_op jit(solution)/shard_map/add | solution.py:233
  321.3 5.2 %convolution_convert_fusion = bf16[640,2048]{1,0:T(8,128)(2,1)S(1)} fusion(bf16[2048,704]{0,1:T(8,128)(2,1)} %all-gather.8.cloned.1.call-done, f32[640,1408]{0,1:T(8,128)} %fusion.14), kind=kOutput, calls=%fused_computation.25 | convolution fusion | flops 1849507840 | bytes 9109504 | tf_op jit(solution)/shard_map/dot_general | solution.py:236
  326.5 0.2 copy.37
  326.7 36.4 %all_to_all.23 = bf16[8,640,256]{2,1,0:T(8,128)(2,1)S(1)} all-to-all(bf16[8,640,256]{2,1,0:T(8,128)(2,1)S(1)} %bitcast.110), channel_id=1, replica_groups=mesh['sp_0'=4,'sp_1'=4,'tp'=8] {'tp'}, dimensions={0} | all-to-all | bytes 5242880 | tf_op jit(solution)/shard_map/all_to_all | solution.py:37
  363.1 0.4 convert_reduce_fusion
  363.5 0.8 fusion.56
  (39 shorter events, 0.1 us)
Async XLA Ops:
  6.5 183.3 %copy-start = (bf16[128,2048]{1,0:T(8,128)(2,1)S(1)}, bf16[128,2048]{1,0:T(8,128)(2,1)}, u32[]{:S(2)}) copy-start(bf16[128,2048]{1,0:T(8,128)(2,1)} %param.23) | copy-start | bytes 1572868
  6.5 7.0 %copy-start.11 = (bf16[128,704]{0,1:T(8,128)(2,1)S(1)}, bf16[128,704]{0,1:T(8,128)(2,1)}, u32[]{:S(2)}) copy-start(bf16[128,704]{0,1:T(8,128)(2,1)} %param.26) | copy-start | bytes 540676
  6.5 7.0 %copy-start.10 = (bf16[128,704]{0,1:T(8,128)(2,1)S(1)}, bf16[128,704]{0,1:T(8,128)(2,1)}, u32[]{:S(2)}) copy-start(bf16[128,704]{0,1:T(8,128)(2,1)} %param.27) | copy-start | bytes 540676
  6.5 7.8 %copy-start.8 = (bf16[640,192]{0,1:T(8,128)(2,1)S(1)}, bf16[640,192]{0,1:T(8,128)(2,1)}, u32[]{:S(2)}) copy-start(bf16[640,192]{0,1:T(8,128)(2,1)} %param.16) | copy-start | bytes 737284
  6.5 84.9 %all-gather.4.cloned.1.call-start = ((), (), s32[]{:S(2)}) async-start(), calls=%async_computation.4 | async-start | bytes 9748480 | tf_op jit(solution)/shard_map/all_gather | solution.py:26
  7.6 6.9 %copy-start.5 = (bf16[640,128]{1,0:T(8,128)(2,1)S(1)}, bf16[640,128]{1,0:T(8,128)(2,1)}, u32[]{:S(2)}) copy-start(bf16[640,128]{1,0:T(8,128)(2,1)} %param.17) | copy-start | bytes 491524
  13.5 261.5 %all-gather.6.cloned.1.call-start = ((), (), s32[]{:S(2)}) async-start(), calls=%async_computation.5 | async-start | bytes 6127616 | tf_op jit(solution)/shard_map/all_gather | solution.py:26
  91.4 14.1 %slice-start = ((s8[9175040]{0:T(1024)(128)(4,1)}), s8[4194304]{0:T(1024)(128)(4,1)S(1)}, s32[]{:S(2)}) async-start(s8[9175040]{0:T(1024)(128)(4,1)} %bitcast.106), calls=%async_computation.7 | async-start | bytes 8388608
  93.5 12.0 %slice-start.1 = ((s8[9175040]{0:T(1024)(128)(4,1)}), s8[4194304]{0:T(1024)(128)(4,1)S(1)}, s32[]{:S(2)}) async-start(s8[9175040]{0:T(1024)(128)(4,1)} %bitcast.106), calls=%async_computation.8 | async-start | bytes 8388608
  93.5 12.0 %slice-start.2 = ((s8[9175040]{0:T(1024)(128)(4,1)}), s8[786432]{0:T(1024)(128)(4,1)S(1)}, s32[]{:S(2)}) async-start(s8[9175040]{0:T(1024)(128)(4,1)} %bitcast.106), calls=%async_computation.9 | async-start | bytes 1572864
  106.1 10.6 %copy-start.2 = (bf16[10240,1,256]{0,2,1:T(8,128)(2,1)}, bf16[10240,1,256]{0,2,1:T(8,128)(2,1)S(1)}, u32[]{:S(2)}) copy-start(bf16[10240,1,256]{0,2,1:T(8,128)(2,1)S(1)} %slice_bitcast_fusion) | copy-start | bytes 15728644
  116.7 18.2 %copy-start.3 = (bf16[640,32]{1,0:T(8,128)(2,1)S(1)}, bf16[640,32]{1,0:T(8,128)(2,1)}, u32[]{:S(2)}) copy-start(bf16[640,32]{1,0:T(8,128)(2,1)} %get-tuple-element.9) | copy-start | bytes 122884
  116.7 18.2 %copy-start.4 = (bf16[640,32]{1,0:T(8,128)(2,1)S(1)}, bf16[640,32]{1,0:T(8,128)(2,1)}, u32[]{:S(2)}) copy-start(bf16[640,32]{1,0:T(8,128)(2,1)} %get-tuple-element.10) | copy-start | bytes 122884
  153.9 16.0 %copy-start.1 = (f32[1,640,10240]{1,2,0:T(8,128)S(1)}, f32[1,640,10240]{1,2,0:T(8,128)}, u32[]{:S(2)}) copy-start(f32[1,640,10240]{1,2,0:T(8,128)} %get-tuple-element.23) | copy-start | bytes 78643200
  169.9 4.2 %copy-start.7 = (bf16[64,2048]{1,0:T(8,128)(2,1)S(1)}, bf16[64,2048]{1,0:T(8,128)(2,1)}, u32[]{:S(2)}) copy-start(bf16[64,2048]{1,0:T(8,128)(2,1)} %param.24) | copy-start | bytes 786436
  206.3 37.2 %copy-start.6 = (bf16[640,256]{1,0:T(8,128)(2,1)S(1)}, bf16[640,256]{1,0:T(8,128)(2,1)}, u32[]{:S(2)}) copy-start(bf16[640,256]{1,0:T(8,128)(2,1)} %param.15) | copy-start | bytes 983044
  243.1 8.7 %copy-start.13 = (f32[256]{0:T(256)S(1)}, f32[256]{0:T(256)}, u32[]{:S(2)}) copy-start(f32[256]{0:T(256)} %param.25) | copy-start | bytes 3076
  252.2 6.7 %copy-start.9 = (bf16[128,704]{0,1:T(8,128)(2,1)S(1)}, bf16[128,704]{0,1:T(8,128)(2,1)}, u32[]{:S(2)}) copy-start(bf16[128,704]{0,1:T(8,128)(2,1)} %param.28) | copy-start | bytes 540676
  254.0 36.9 %all-to-all-start.2 = ((bf16[8,640,256]{1,2,0:T(8,128)(2,1)}), bf16[8,640,256]{1,2,0:T(8,128)(2,1)}, u32[]{:S(2)}, u32[]{:S(2)}) async-start(bf16[8,640,256]{1,2,0:T(8,128)(2,1)} %broadcast_in_dim.5), calls=%async_computation.2 | async-start | bytes 5242880 | tf_op jit(solution)/shard_map/all_to_all | solution.py:43
  258.9 62.4 %all-gather.8.cloned.1.call-start = ((), (), s32[]{:S(2)}) async-start(), calls=%async_computation.6 | async-start | bytes 3604480 | tf_op jit(solution)/shard_map/all_gather | solution.py:66
  290.9 5.2 %copy-start.14 = (bf16[2048,1408]{0,1:T(8,128)(2,1)S(1)}, bf16[2048,1408]{0,1:T(8,128)(2,1)}, u32[]{:S(2)}) copy-start(bf16[2048,1408]{0,1:T(8,128)(2,1)} %all-gather.6.cloned.1.call-done) | copy-start | bytes 17301508
  296.1 9.5 %copy-start.12 = (f32[3,2,704]{2,1,0:T(2,128)S(1)}, f32[3,2,704]{2,1,0:T(2,128)}, u32[]{:S(2)}) copy-start(f32[3,2,704]{2,1,0:T(2,128)} %param.29) | copy-start | bytes 50692
  300.5 9.9 %collective-permute-start = (bf16[1,1408]{0,1:T(8,128)(2,1)S(1)}, bf16[1,1408]{0,1:T(8,128)(2,1)}, u32[]{:S(2)}, u32[]{:S(2)}) collective-permute-start(bf16[1,1408]{0,1:T(8,128)(2,1)S(1)} %get-tuple-element.7), channel_id=1, source_target_pairs={{0,8},{8,16},{16,24},{24,32},{32,40},{40,48},{48,56},{56,64},{64,7... | collective-permute-start | bytes 8456 | tf_op jit(solution)/shard_map/ppermute | solution.py:75
  304.4 10.7 %collective-permute-start.1 = (bf16[1,1408]{0,1:T(8,128)(2,1)S(1)}, bf16[1,1408]{0,1:T(8,128)(2,1)}, u32[]{:S(2)}, u32[]{:S(2)}) collective-permute-start(bf16[1,1408]{0,1:T(8,128)(2,1)S(1)} %get-tuple-element.8), channel_id=1, source_target_pairs={{8,0},{16,8},{24,16},{32,24},{40,32},{48,40},{56,48},{64,56},{72,6... | collective-permute-start | bytes 8456 | tf_op jit(solution)/shard_map/ppermute | solution.py:78
Sparse Core Ops, SparseCore 0:
  13.6 77.7 all-gather.3
  93.5 62.8 all-gather.5
  275.1 41.2 all-gather.7
where the time goes:
time: 372 us; the launch traced here: 371 us
  matrix products  110 us (30%)
  waiting for transfers between devices  99.6 us (27%)
  blocking collectives  97.3 us (26%)
  other arithmetic  30 us (8%)
  between operations  13.5 us (4%)
  local copies, waits for them, and re-layouts  10.7 us (3%)
  starting transfers between devices  10.2 us (3%)
    all_gather x2, waiting for transfers between devices, sent_together(): lax.all_gather(both, axis, axis=dim, tiled=True)  74.5 us
    all_to_all x2, blocking collectives, sum_at_owner(): lax.all_to_all(in_blocks(shard, dim, count), axis, 0, 0, tiled=True)  73.2 us
    dot_general x2, matrix products, attend_piece(): jnp.einsum('qhd,kd->hqk', query_turned[..., nope_dim:], rope_piece, prefe...  37.2 us
    dot_general x2, matrix products, attend_piece(): jnp.einsum('qhd,khd->hqk', query_turned[..., :nope_dim], kv_piece[..., :n...  22.6 us
    dot_general x1, matrix products, per_device(): jnp.dot(heads_wide, out_wide, preferred_element_type=jnp.float32)  16.3 us
    all_gather x1, blocking collectives, gathered_by_axis(): nearer = lax.all_gather(shard, axes[-1], axis=dim, tiled=True)  16 us
    all_to_all x1, waiting for transfers between devices, from_everyone(): lax.all_to_all(jnp.broadcast_to(shard[None], (count, *shard.shape)), axis...  15.9 us
    dot_general x1, matrix products, per_device(): jnp.dot(heads_narrow, out_narrow, preferred_element_type=jnp.float32)  15.7 us
  transfers between devices with their start and end apart: 6, of which 4 were waited for; matrix products, arithmetic and copies ran while one was open for 35% of the time, Pallas kernels for 0%

commit v1 on v0

v1 whole, which is shorter than its diff:
```python
import jax
import jax.numpy as jnp
from jax import lax
from jax.experimental import pallas as pl
from jax.experimental.pallas import tpu as pltpu
from jax.sharding import PartitionSpec as P

D = 2048
FF = 5632
RANK = 512
ROPE = 64
NOPE_W = 128
VAL_W = 128
NOPE_N = 64
VAL_N = 64
N_TP = 8
N_SP = 16
ROWS = 640
UNITS = FF // N_TP
FEATS = D // N_TP
EDGE = 16

theta = 10000.0
epsilon = 1e-06
LOG2E = 1.4426950408889634
SCALE_W = (NOPE_W + ROPE) ** -0.5 * LOG2E
SCALE_N = (NOPE_N + ROPE) ** -0.5 * LOG2E

MESH = pl.DeviceIdType.MESH
F32 = jnp.float32
BF16 = jnp.bfloat16

ORDER = (
    (0, 0), (1, 0), (3, 0), (0, 1), (0, 3), (2, 0), (1, 1), (1, 3),
    (3, 1), (3, 3), (0, 2), (2, 1), (2, 3), (1, 2), (3, 2), (2, 2),
)
SLOT = {offset: index for index, offset in enumerate(ORDER)}
PAIRS = len(ORDER) // 2
KEYS = 1280
CHUNK = 128


def rotate(values, positions):
    half_dim = values.shape[-1] // 2
    inverse = jnp.power(
        jnp.float32(theta), -2.0 * jnp.arange(half_dim, dtype=jnp.float32) / values.shape[-1]
    )
    angles = positions[:, None] * inverse[None, :]
    cosine = jnp.cos(angles)
    sine_part = jnp.sin(angles)
    floats = values.astype(jnp.float32)
    lower_half = floats[..., :half_dim]
    upper_half = floats[..., half_dim:]
    turned = jnp.concatenate(
        [
            lower_half * cosine - upper_half * sine_part,
            lower_half * sine_part + upper_half * cosine,
        ],
        axis=-1,
    )
    return turned.astype(jnp.bfloat16)


class Place:
    def __init__(self):
        self.sp = lax.axis_index("sp")
        self.tp = lax.axis_index("tp")
        self.z, self.y = lax.div(self.sp, 4), lax.rem(self.sp, 4)
        self.x, self.c = lax.div(self.tp, 2), lax.rem(self.tp, 2)

    def along(self, first, second):
        z = lax.rem(self.z + first * (1 - self.c) + second * self.c, 4)
        y = lax.rem(self.y + first * self.c + second * (1 - self.c), 4)
        return z * 4 + y

    def device(self, first, second):
        return {"sp": self.along(first, second), "tp": self.tp}

    def feature(self, dx, other=0):
        core = self.c if not other else 1 - self.c
        return lax.rem(self.x + dx, 4) * 2 + core

    def peer(self, dx, other=0):
        return {"sp": self.sp, "tp": self.feature(dx, other)}


class Copies:
    def __init__(self):
        self.sent = []

    def start(self, build):
        def copy():
            src, dst, send, recv, device = build()
            return pltpu.make_async_remote_copy(
                src_ref=src, dst_ref=dst, send_sem=send, recv_sem=recv, device_id=device, device_id_type=MESH
            )

        copy().start()
        self.sent.append(copy)

    def arrived(self, dst, recv, device):
        pltpu.make_async_remote_copy(
            src_ref=dst, dst_ref=dst, send_sem=recv, recv_sem=recv, device_id=device, device_id_type=MESH
        ).wait_recv()

    def drain(self):
        for copy in self.sent:
            copy().wait_send()
        self.sent = []


def onward(offset):
    df, ds = offset
    moves = []
    if ds == 0:
        if df == 3:
            moves.append((1, 0, 0, (2, 0)))
        if df == 1:
            moves.append((3, 0, 1, (2, 0)))
        if df == 0:
            moves.append((1, 0, None, (3, 0)))
            moves.append((3, 0, None, (1, 0)))
        moves.append((0, 1, None, (df, 3)))
        moves.append((0, 3, None, (df, 1)))
    elif ds == 3:
        moves.append((0, 1, 0, (df, 2)))
    elif ds == 1:
        moves.append((0, 3, 1, (df, 2)))
    return moves


MOVES = [(offset, move) for offset in ORDER for move in onward(offset)]
SEND = {key: index for index, key in enumerate(MOVES)}
N_SEND = len(MOVES)


class Gather:
    def __init__(self, copies, place, view, send, recv, own=None):
        self.copies, self.place, self.view = copies, place, view
        self.send, self.recv, self.own = send, recv, own

    def forward(self, offset):
        for move in onward(offset):
            for part in range(self.send.shape[0]):
                self.copies.start(lambda move=move, part=part: self._copy(offset, move, part))

    def _copy(self, offset, move, part):
        first, second, half, target = move
        source = self.own(half) if offset == (0, 0) and self.own else self.view(offset, half)
        return (
            source[part],
            self.landing(offset, target, half)[part],
            self.send.at[part, SEND[(offset, move)]],
            self.recv.at[part, SLOT[target] * 2 + (half or 0)],
            self.place.device(first, second),
        )

    def landing(self, offset, target, half):
        return self.view(target, half)

    def wait(self, offset):
        if offset == (0, 0):
            return
        halves = (0, 1) if 2 in offset and not (offset[0] == 2 and offset[1] in (1, 3)) else (None,)
        for half in halves:
            for part, dst in enumerate(self.view(offset, half)):
                self.copies.arrived(
                    dst, self.recv.at[part, SLOT[offset] * 2 + (half or 0)], self.place.device(0, 1)
                )


class GatherPlaced(Gather):
    def landing(self, offset, target, half):
        return self.view(offset, half)


class RingGather:
    def __init__(self, copies, place, view, send, recv):
        self.copies, self.place, self.view = copies, place, view
        self.send, self.recv = send, recv

    def _send(self, feature, half, index, arrival, device):
        for part, ref in enumerate(self.view(feature, half)):
            self.copies.start(
                lambda part=part, ref=ref: (ref, ref, self.send.at[part, index], self.recv.at[part, arrival], device)
            )

    def _wait(self, feature, half, arrival):
        for part, ref in enumerate(self.view(feature, half)):
            self.copies.arrived(ref, self.recv.at[part, arrival], self.place.peer(0, 1))

    def begin(self):
        place = self.place
        me = place.feature(0)
        self._send(me, None, 0, 0, place.peer(1))
        self._send(me, None, 1, 1, place.peer(3))
        self._send(me, None, 2, 4, place.peer(0, 1))

    def middle(self):
        place = self.place
        left, right = place.feature(3), place.feature(1)
        self._wait(left, None, 0)
        self._send(left, 0, 3, 2, place.peer(1))
        self._send(left, None, 4, 5, place.peer(0, 1))
        self._wait(right, None, 1)
        self._send(right, 1, 5, 3, place.peer(3))
        self._send(right, None, 6, 6, place.peer(0, 1))

    def end(self):
        place = self.place
        far = place.feature(2)
        self._wait(far, 0, 2)
        self._wait(far, 1, 3)
        self._send(far, None, 7, 7, place.peer(0, 1))
        self._wait(place.feature(0, 1), None, 4)
        self._wait(place.feature(3, 1), None, 5)
        self._wait(place.feature(1, 1), None, 6)
        self._wait(place.feature(2, 1), None, 7)


def half_rows(half, rows, start=0):
    if half is None:
        return pl.ds(start, rows)
    return pl.ds(start + half * (rows // 2), rows // 2)


def kernel(
    qw_ref, qn_ref, lat_ref, rope_ref, ew_ref, en_ref, res_ref, ow_ref, on_ref, gain_ref, up_ref, dn_ref, taps_ref,
    out_ref,
    latb, ropb, upf, dnf, kbuf, vbuf, mrow, lrow, acc, hw, hn, oww, ownr, own0, own1, gains, att, nrm, upx, hid,
    part, send_a, recv_a, send_b, recv_b, send_c, recv_c,
    ls, lr, lps, lpr, us, ur, ds_, dr, hs, hr, as_, ar, xs, xr, es, er, rs, rr,
):
    place = Place()
    copies = Copies()
    c, tp, sp = place.c, place.tp, place.sp

    barrier = pltpu.get_barrier_semaphore()
    talk = [place.device(f, s) for f, s in ((1, 0), (3, 0), (0, 1), (0, 3))]
    talk += [{"sp": sp, "tp": lax.rem(tp + d, N_TP)} for d in range(1, N_TP)]
    talk += [{"sp": lax.rem(sp + d, N_SP), "tp": tp} for d in (1, N_SP - 1)]
    for device in talk:
        pl.semaphore_signal(barrier, inc=1, device_id=device, device_id_type=MESH)
    pl.semaphore_wait(barrier, len(talk))

    lat_gather = Gather(
        copies,
        place,
        lambda offset, half: [
            latb.at[c, SLOT[offset], half_rows(half, 320)],
            ropb.at[c, SLOT[offset], half_rows(half, 160)],
        ],
        ls,
        lr,
        own=lambda half: [lat_ref.at[c, half_rows(half, 320)], rope_ref.at[c, half_rows(half, 160)]],
    )

    def up_view(offset, half):
        origin = place.along(*offset)
        return [upf.at[half_rows(half, 128, origin * 128)]]

    def dn_view(offset, half):
        origin = place.along(*offset)
        return [dnf.at[half_rows(half, 128, origin * 128)]]

    up_gather = GatherPlaced(copies, place, up_view, us, ur, own=lambda half: [up_ref.at[half_rows(half, 128)]])
    dn_gather = GatherPlaced(copies, place, dn_view, ds_, dr, own=lambda half: [dn_ref.at[half_rows(half, 128)]])

    lat_gather.forward((0, 0))

    def exchange(d, start):
        to, source = lax.rem(tp + d, N_TP), lax.rem(tp + N_TP - d, N_TP)
        arrays = (
            (ow_ref.at[:, pl.ds(pl.multiple_of(to * FEATS, FEATS), FEATS)], oww.at[tp], oww.at[source]),
            (on_ref.at[:, pl.ds(pl.multiple_of(to * FEATS, FEATS), FEATS)], ownr.at[tp], ownr.at[source]),
            (gain_ref, gains.at[tp], gains.at[source]),
        )
        for index, (src, dst, landed) in enumerate(arrays):
            if start:
                copies.start(
                    lambda src=src, dst=dst, index=index: (
                        src, dst, xs.at[index, d], xr.at[index, d], {"sp": sp, "tp": to}
                    )
                )
            else:
                copies.arrived(landed, xr.at[index, d], {"sp": sp, "tp": to})

    for d in range(1, N_TP):
        exchange(d, True)

    mine = pl.ds(pl.multiple_of(tp * FEATS, FEATS), FEATS)
    oww[tp] = ow_ref[:, mine]
    ownr[tp] = on_ref[:, mine]
    gains[tp] = gain_ref[...]
    upf[pl.ds(sp * 128, 128), :] = up_ref[...]
    dnf[pl.ds(sp * 128, 128), :] = dn_ref[...]
    for half in range(2):
        latb[half, 0] = lat_ref[half]
        ropb[half, 0] = rope_ref[half]

    mrow[...] = jnp.full_like(mrow, -1e30)
    lrow[...] = jnp.zeros_like(lrow)
    acc[...] = jnp.zeros_like(acc)

    def partner_view(core, slot):
        return [latb.at[core, slot], ropb.at[core, slot]]

    def attention_step(pair, carry):
        for k in range(PAIRS):

            @pl.when(pair == k)
            def _():
                for slot in (2 * k, 2 * k + 1):
                    offset = ORDER[slot]
                    if slot == 0:
                        continue
                    lat_gather.wait(offset)
                    lat_gather.forward(offset)
                    for index in range(2):
                        copies.start(
                            lambda index=index, slot=slot: (
                                partner_view(c, slot)[index], partner_view(c, slot)[index],
                                lps.at[index, slot], lpr.at[index, slot], place.peer(0, 1),
                            )
                        )
                if k == 6:
                    up_gather.forward((0, 0))
                if k == 7:
                    dn_gather.forward((0, 0))
                for slot in (2 * k, 2 * k + 1):
                    if slot:
                        for index, ref in enumerate(partner_view(1 - c, slot)):
                            copies.arrived(ref, lpr.at[index, slot], place.peer(0, 1))

        lane = lax.broadcasted_iota(jnp.int32, (160, 128), 1)
        for u in range(4):
            block = latb[u % 2, 2 * pair + u // 2]
            turned = ropb[u % 2, 2 * pair + u // 2].astype(F32)
            wide = jnp.dot(block, ew_ref[...], preferred_element_type=F32)
            narrow = jnp.dot(block, en_ref[...], preferred_element_type=F32)
            rows = pl.ds(u * 320, 320)
            kbuf[rows, 0:128] = wide[:, :128].astype(BF16)
            vbuf[rows, 0:128] = wide[:, 128:].astype(BF16)
            vbuf[rows, 128:256] = narrow.astype(BF16)
            kbuf[pl.ds(u * 320, 160), 128:256] = jnp.where(
                lane < 64, narrow[:160], pltpu.roll(turned, 64, 1)
            ).astype(BF16)
            kbuf[pl.ds(u * 320 + 160, 160), 128:256] = jnp.where(lane < 64, narrow[160:], turned).astype(BF16)

        def chunk_step(index, inner):
            for group in range(2):
                q_ref, lanes, scale = (qw_ref, slice(0, 256), SCALE_W) if group == 0 else (qn_ref, slice(128, 256), SCALE_N)
                q_rows = pl.ds(index * CHUNK, CHUNK)
                rows = pl.ds(group * ROWS + index * CHUNK, CHUNK)
                scores = lax.dot_general(
                    q_ref[q_rows, :], kbuf[:, lanes], (((1,), (1,)), ((), ())), preferred_element_type=F32
                )
                before = mrow[rows, 0:1]
                top = jnp.maximum(before, jnp.max(scores, axis=1, keepdims=True))
                weights = jnp.exp2((scores - top) * scale)
                shrink = jnp.exp2((before - top) * scale)
                total = shrink * lrow[rows, 0:1] + jnp.sum(weights, axis=1, keepdims=True)
                values = jnp.dot(
                    weights.astype(BF16), vbuf[:, group * 128 : group * 128 + 128], preferred_element_type=F32
                )
                acc[rows, :] = shrink * acc[rows, :] + values
                mrow[rows, :] = jnp.broadcast_to(top, (CHUNK, 128))
                lrow[rows, :] = jnp.broadcast_to(total, (CHUNK, 128))
            return inner

        lax.fori_loop(0, ROWS // CHUNK, chunk_step, 0)
        return carry

    lax.fori_loop(0, PAIRS, attention_step, 0)

    hw[tp] = (acc[0:ROWS, :] / lrow[0:ROWS, :]).astype(BF16)
    low = acc[ROWS : ROWS + 320, :] / lrow[ROWS : ROWS + 320, :]
    high = acc[ROWS + 320 : 2 * ROWS, :] / lrow[ROWS + 320 : 2 * ROWS, :]
    lane = lax.broadcasted_iota(jnp.int32, (320, 128), 1)
    hn[tp] = jnp.where(lane < 64, pltpu.roll(low, 64, 1), high).astype(BF16)
    head_gather = RingGather(
        copies,
        place,
        lambda feature, half: [hw.at[feature, half_rows(half, 640)], hn.at[feature, half_rows(half, 320)]],
        hs,
        hr,
    )
    head_gather.begin()

    for offset in ((1, 0), (3, 0), (0, 1), (0, 3)):
        up_gather.wait(offset)
        up_gather.forward(offset)

    for d in range(1, N_TP):
        exchange(d, False)
    zero = jnp.zeros((64, FEATS), BF16)
    for j in range(N_TP):
        own0[pl.ds(j * 128, 64), :] = ownr[j]
        own0[pl.ds(j * 128 + 64, 64), :] = zero
        own1[pl.ds(j * 128, 64), :] = zero
        own1[pl.ds(j * 128 + 64, 64), :] = ownr[j]

    head_gather.middle()
    for offset in ((2, 0), (1, 1), (1, 3), (3, 1), (3, 3)):
        up_gather.wait(offset)
        up_gather.forward(offset)
    for offset in ((1, 0), (3, 0), (0, 1), (0, 3)):
        dn_gather.wait(offset)
        dn_gather.forward(offset)
    head_gather.end()

    wide_heads = jnp.concatenate([hw[j] for j in range(N_TP)], axis=1)
    narrow_heads = jnp.concatenate([hn[j] for j in range(N_TP)], axis=1)
    summed = jnp.dot(wide_heads, oww[...].reshape(N_TP * 128, FEATS), preferred_element_type=F32)
    top = jnp.dot(narrow_heads, own0[...], preferred_element_type=F32)
    bottom = jnp.dot(narrow_heads, own1[...], preferred_element_type=F32)
    att[tp, 0:320] = (res_ref[0:320, :].astype(F32) + summed[0:320] + top).astype(BF16)
    att[tp, 320:640] = (res_ref[320:640, :].astype(F32) + summed[320:640] + bottom).astype(BF16)

    att_gather = RingGather(
        copies, place, lambda feature, half: [att.at[feature, half_rows(half, 640)]], as_, ar
    )
    att_gather.begin()
    for offset in ((0, 2), (2, 1), (2, 3)):
        up_gather.wait(offset)
        up_gather.forward(offset)
    att_gather.middle()
    for offset in ((1, 2), (3, 2), (2, 2)):
        up_gather.wait(offset)
        up_gather.forward(offset)
    for offset in ((2, 0), (1, 1), (1, 3), (3, 1), (3, 3)):
        dn_gather.wait(offset)
        dn_gather.forward(offset)
    att_gather.end()

    def norm_step(index, carry):
        rows = pl.ds(index * 64, 64)
        squares = jnp.zeros((64, FEATS), F32)
        for j in range(N_TP):
            piece = att[j, rows, :].astype(F32)
            squares = squares + piece * piece
        factor = lax.rsqrt(jnp.sum(squares, axis=1, keepdims=True) * (1.0 / D) + epsilon)
        for j in range(N_TP):
            nrm[rows, j * FEATS : (j + 1) * FEATS] = (
                att[j, rows, :].astype(F32) * factor * gains[j, 0:1, :]
            ).astype(BF16)
        return carry

    lax.fori_loop(0, ROWS // 64, norm_step, 0)

    def up_step(index, carry):
        columns = pl.ds(pl.multiple_of(index * 256, 256), 256)
        upx[EDGE : EDGE + ROWS, columns] = jnp.dot(
            nrm[...], upf[:, columns], preferred_element_type=F32
        ).astype(BF16)
        return carry

    lax.fori_loop(0, 5, up_step, 0)
    upx[EDGE : EDGE + ROWS, 1280:1408] = jnp.dot(nrm[...], upf[:, 1280:1408], preferred_element_type=F32).astype(BF16)

    following = {"sp": lax.rem(sp + 1, N_SP), "tp": tp}
    leading = {"sp": lax.rem(sp + N_SP - 1, N_SP), "tp": tp}
    copies.start(lambda: (upx.at[pl.ds(ROWS, EDGE)], upx.at[pl.ds(0, EDGE)], es.at[0], er.at[0], following))
    copies.start(lambda: (upx.at[pl.ds(EDGE, EDGE)], upx.at[pl.ds(ROWS + EDGE, EDGE)], es.at[1], er.at[1], leading))
    for offset in ((0, 2), (2, 1), (2, 3)):
        dn_gather.wait(offset)
        dn_gather.forward(offset)
    copies.arrived(upx.at[pl.ds(0, EDGE)], er.at[0], following)
    copies.arrived(upx.at[pl.ds(ROWS + EDGE, EDGE)], er.at[1], leading)

    def conv_step(index, carry):
        span = pl.ds(index * 128, 160)
        position = lax.broadcasted_iota(jnp.int32, (160, 1), 0) + index * 128 - EDGE
        outside = ((sp == 0) & (position < 0)) | ((sp == N_SP - 1) & (position >= ROWS))

        def smooth(columns):
            wide = jnp.where(outside, 0.0, upx[span, columns].astype(F32))
            low = pltpu.roll(wide, 1, 0)[16:144]
            high = pltpu.roll(wide, 159, 0)[16:144]
            return taps_ref[0:1, columns] * low + taps_ref[1:2, columns] * wide[16:144] + taps_ref[2:3, columns] * high

        def gated(gate, value):
            return gate / (1.0 + jnp.exp(-gate)) * value

        rows = pl.ds(index * 128, 128)
        for n in range(5):
            gate = smooth(slice(n * 128, n * 128 + 128))
            value = smooth(slice(640 + n * 128, 640 + n * 128 + 128))
            hid[rows, n * 128 : n * 128 + 128] = gated(gate, value).astype(BF16)
        both = smooth(slice(1280, 1408))
        hid[rows, 640:704] = gated(both, pltpu.roll(both, 64, 1))[:, :64].astype(BF16)
        return carry

    lax.fori_loop(0, 5, conv_step, 0)

    for offset in ((1, 2), (3, 2), (2, 2)):
        dn_gather.wait(offset)
        dn_gather.forward(offset)

    def down(feature):
        return lax.dot_general(
            hid[...], dnf[pl.ds(pl.multiple_of(feature * FEATS, FEATS), FEATS), :], (((1,), (1,)), ((), ())),
            preferred_element_type=F32,
        )

    for dx in (2, 1, 3, 0):
        send_a[dx] = down(place.feature(dx, 1)).astype(BF16)
        copies.start(lambda dx=dx: (send_a.at[dx], recv_a.at[dx], rs.at[dx], rr.at[dx], place.peer(0, 1)))
        part[dx] = down(place.feature(dx))

    def pair_sum(dx):
        copies.arrived(recv_a.at[dx], rr.at[dx], place.peer(0, 1))
        return part[dx] + recv_a[dx].astype(F32)

    far = pair_sum(2)
    send_b[0] = far[0:320].astype(BF16)
    send_b[1] = far[320:640].astype(BF16)
    copies.start(lambda: (send_b.at[0], recv_b.at[0], rs.at[4], rr.at[4], place.peer(1)))
    copies.start(lambda: (send_b.at[1], recv_b.at[1], rs.at[5], rr.at[5], place.peer(3)))
    right = pair_sum(1)
    left = pair_sum(3)
    send_c[0, 320:640] = right[320:640].astype(BF16)
    send_c[1, 0:320] = left[0:320].astype(BF16)
    copies.start(lambda: (send_c.at[0, pl.ds(320, 320)], recv_c.at[0, pl.ds(320, 320)], rs.at[6], rr.at[6], place.peer(1)))
    copies.start(lambda: (send_c.at[1, pl.ds(0, 320)], recv_c.at[1, pl.ds(0, 320)], rs.at[7], rr.at[7], place.peer(3)))
    copies.arrived(recv_b.at[0], rr.at[4], place.peer(1))
    send_c[0, 0:320] = (right[0:320] + recv_b[0].astype(F32)).astype(BF16)
    copies.start(lambda: (send_c.at[0, pl.ds(0, 320)], recv_c.at[0, pl.ds(0, 320)], rs.at[8], rr.at[8], place.peer(1)))
    copies.arrived(recv_b.at[1], rr.at[5], place.peer(3))
    send_c[1, 320:640] = (left[320:640] + recv_b[1].astype(F32)).astype(BF16)
    copies.start(lambda: (send_c.at[1, pl.ds(320, 320)], recv_c.at[1, pl.ds(320, 320)], rs.at[9], rr.at[9], place.peer(3)))
    own_sum = pair_sum(0) + att[tp].astype(F32)
    copies.arrived(recv_c.at[0, pl.ds(320, 320)], rr.at[6], place.peer(1))
    copies.arrived(recv_c.at[1, pl.ds(0, 320)], rr.at[7], place.peer(1))
    copies.arrived(recv_c.at[0, pl.ds(0, 320)], rr.at[8], place.peer(1))
    copies.arrived(recv_c.at[1, pl.ds(320, 320)], rr.at[9], place.peer(1))
    out_ref[...] = (own_sum + recv_c[0].astype(F32) + recv_c[1].astype(F32)).astype(BF16)
    copies.drain()


def per_device(
    residual, query_wide, query_narrow, latent, rope_key, latent_gain, expand_wide, expand_narrow,
    out_wide, out_narrow, norm_gain, up_gate, up_value, down_weight, conv_taps,
):
    offset = lax.axis_index("sp") * ROWS
    positions = (offset + lax.iota(jnp.int32, ROWS)).astype(jnp.float32)
    latent_float = latent.astype(jnp.float32)
    normed_latent = (
        latent_float
        * lax.rsqrt(jnp.mean(latent_float * latent_float, axis=-1, keepdims=True) + epsilon)
        * latent_gain
    ).astype(jnp.bfloat16)
    rope_turned = rotate(rope_key, positions)
    blank = jnp.zeros((ROWS, 64), BF16)
    q_wide = jnp.concatenate(
        [query_wide[:, :NOPE_W], blank, rotate(query_wide[:, NOPE_W:], positions)], axis=1
    )
    q_narrow = jnp.concatenate([query_narrow[:, :NOPE_N], rotate(query_narrow[:, NOPE_N:], positions)], axis=1)
    rope_packed = rope_turned.reshape(2, 2, 160, ROPE).transpose(0, 2, 1, 3).reshape(2, 160, 2 * ROPE)

    def interleave(gate, value):
        return jnp.concatenate(
            [gate[:, :640], value[:, :640], gate[:, 640:], value[:, 640:]], axis=1
        )

    up_block = interleave(up_gate, up_value)
    taps = interleave(conv_taps[:, 0], conv_taps[:, 1])
    gain = jnp.broadcast_to(norm_gain[None, :], (8, FEATS))
    vmem = pl.BlockSpec(memory_space=pltpu.VMEM)
    dma = pltpu.SemaphoreType.DMA
    return pl.pallas_call(
        kernel,
        out_shape=jax.ShapeDtypeStruct((ROWS, FEATS), BF16),
        in_specs=[vmem] * 13,
        out_specs=vmem,
        scratch_shapes=[
            pltpu.VMEM((2, 16, 320, RANK), BF16),
            pltpu.VMEM((2, 16, 160, 128), BF16),
            pltpu.VMEM((D, 2 * UNITS), BF16),
            pltpu.VMEM((D, UNITS), BF16),
            pltpu.VMEM((KEYS, 256), BF16),
            pltpu.VMEM((KEYS, 256), BF16),
            pltpu.VMEM((2 * ROWS, 128), F32),
            pltpu.VMEM((2 * ROWS, 128), F32),
            pltpu.VMEM((2 * ROWS, 128), F32),
            pltpu.VMEM((N_TP, ROWS, 128), BF16),
            pltpu.VMEM((N_TP, ROWS // 2, 128), BF16),
            pltpu.VMEM((N_TP, 128, FEATS), BF16),
            pltpu.VMEM((N_TP, 64, FEATS), BF16),
            pltpu.VMEM((N_TP * 128, FEATS), BF16),
            pltpu.VMEM((N_TP * 128, FEATS), BF16),
            pltpu.VMEM((N_TP, 8, FEATS), F32),
            pltpu.VMEM((N_TP, ROWS, FEATS), BF16),
            pltpu.VMEM((ROWS, D), BF16),
            pltpu.VMEM((ROWS + 2 * EDGE, 2 * UNITS), BF16),
            pltpu.VMEM((ROWS, UNITS), BF16),
            pltpu.VMEM((4, ROWS, FEATS), F32),
            pltpu.VMEM((4, ROWS, FEATS), BF16),
            pltpu.VMEM((4, ROWS, FEATS), BF16),
            pltpu.VMEM((2, ROWS // 2, FEATS), BF16),
            pltpu.VMEM((2, ROWS // 2, FEATS), BF16),
            pltpu.VMEM((2, ROWS, FEATS), BF16),
            pltpu.VMEM((2, ROWS, FEATS), BF16),
            dma((2, N_SEND)), dma((2, 32)), dma((2, 16)), dma((2, 16)),
            dma((1, N_SEND)), dma((1, 32)),
            dma((1, N_SEND)), dma((1, 32)),
            dma((2, 8)), dma((2, 8)),
            dma((1, 8)), dma((1, 8)),
            dma((3, 8)), dma((3, 8)),
            dma((2,)), dma((2,)),
            dma((10,)), dma((10,)),
        ],
        compiler_params=pltpu.CompilerParams(
            collective_id=0, has_side_effects=True, vmem_limit_bytes=67043328
        ),
    )(
        q_wide, q_narrow, normed_latent.reshape(2, 320, RANK), rope_packed, expand_wide, expand_narrow,
        residual, out_wide, out_narrow, gain, up_block, down_weight, taps,
    )


def solution(mesh):
    in_specs = (
        P("sp", "tp"), P("sp", "tp"), P("sp", "tp"), P("sp", None), P("sp", None), P(),
        P(None, "tp"), P(None, "tp"), P("tp", None), P("tp", None), P("tp"),
        P("sp", "tp"), P("sp", "tp"), P("sp", "tp"), P(None, None, "tp"),
    )
    return jax.shard_map(
        per_device, mesh=mesh, in_specs=in_specs, out_specs=P("sp", "tp"), check_vma=False
    )
```

time: 372 us -> 176 us (0.47)
  Pallas kernels: 0 us -> 162 us
  matrix products: 110 us -> 0 us
  waiting for transfers between devices: 99.6 us -> 0 us
  blocking collectives: 97.3 us -> 0 us
  other arithmetic: 30 us -> 4.84 us
  between operations: 13.5 us -> 0.23 us
  starting transfers between devices: 10.2 us -> 0 us
    pallas_call x0 -> x1, Pallas kernels: none -> 162 us  [per_device(): pl.pallas_call(kernel, out_shape=jax.ShapeDtypeStruct((ROWS, FEATS), BF16...]
    dot_general x11 -> x0, matrix products: 110 us -> none  [the longest x2 37.2 us: attend_piece(): jnp.einsum('qhd,kd->hqk', query_turned[..., nope_dim:], rope_piece, prefe...]
    all_to_all x3 -> x0, blocking collectives: 81.2 us -> none  [the longest x2 73.2 us: sum_at_owner(): lax.all_to_all(in_blocks(shard, dim, count), axis, 0, 0, tiled=True)]
    all_gather x3 -> x0, waiting for transfers between devices: 74.5 us -> none  [the longest x2 74.5 us: sent_together(): lax.all_gather(both, axis, axis=dim, tiled=True)]
    all_gather x1 -> x0, blocking collectives: 16 us -> none  [gathered_by_axis(): nearer = lax.all_gather(shard, axes[-1], axis=dim, tiled=True)]
    all_to_all x1 -> x0, waiting for transfers between devices: 15.9 us -> none  [from_everyone(): lax.all_to_all(jnp.broadcast_to(shard[None], (count, *shard.shape)), axis...]
    reduce_sum x6 -> x0, other arithmetic: 15.8 us -> none  [the longest x2 14.8 us: attend_piece(): row_total = jnp.sum(weights, axis=-1)]
    ppermute x2 -> x0, waiting for transfers between devices: 9.15 us -> none  [the longest x1 4.67 us: padded(): lax.ppermute(lax.slice_in_dim(block, 0, width, axis=dim), axis, backward)]
  transfers between devices with their start and end apart: 6 -> 0, of which waited for: 4 -> 0; matrix products, arithmetic and copies ran while one was open for 35% -> 0% of each run, Pallas kernels for 0% -> 0%
where the time goes in v1:
time: 176 us
  Pallas kernels  162 us (92%)
  local copies, waits for them, and re-layouts  8.72 us (5%)
  other arithmetic  4.84 us (3%)
    pallas_call x1, Pallas kernels, per_device(): pl.pallas_call(kernel, out_shape=jax.ShapeDtypeStruct((ROWS, FEATS), BF16...  162 us
    unnamed x21, local copies, waits for them, and re-layouts  5.17 us

profile of v1, /device:TPU:1, one launch (start us, length us, event | category | flops | bytes accessed | tf_op | source)
XLA Modules:
  0.0 176.0 jit_solution(15210558001321569915)
XLA Ops:
  0.0 0.0 slice-start
  0.0 1.1 copy.44
  1.1 0.0 copy-start.1
  1.2 0.0 slice-done
  1.2 0.2 copy.56
  1.4 0.6 copy-done.1
  2.0 0.1 fusion.27
  2.1 0.0 slice-start.1
  2.1 1.6 fusion.24
  3.8 0.0 slice-done.1
  3.8 0.2 copy.55
  4.0 0.0 copy-start
  4.0 0.9 pad_maximum_fusion.qw_ref
  4.9 0.0 copy-start.4
  4.9 0.8 pad_maximum_fusion.1.qn_ref
  5.7 0.0 copy-done
  5.7 0.2 fusion
  5.9 0.0 copy-done.4
  5.9 1.1 fusion.2
  7.0 0.0 copy-start.5
  7.0 0.0 slice-start.2
  7.0 0.1 copy.46
  7.1 0.1 copy.45
  7.3 0.0 slice-start.4
  7.3 0.7 copy.53.rope_ref
  8.0 0.0 copy-done.5
  8.0 0.6 broadcast_in_dim.5.gain_ref
  8.6 0.0 slice-start.3
  8.6 0.0 slice-start.5
  8.6 0.0 slice-done.2
  8.6 0.2 copy.57
  8.8 0.0 slice-done.4
  8.8 0.0 copy-start.2
  8.8 0.2 copy.58
  9.0 0.0 copy-start.3
  9.0 0.4 slice-done.3
  9.3 0.1 copy.59
  9.5 0.0 slice-done.5
  9.5 0.1 copy.60
  9.6 0.9 concatenate.32.up_ref
  10.5 0.0 copy-done.2
  10.5 0.8 copy.54.dn_ref
  11.3 0.0 copy-done.3
  11.4 0.7 concatenate.33.taps_ref
  12.1 162.2 %shard_map.145 = bf16[640,256]{1,0:T(8,128)(2,1)} custom-call(bf16[640,256]{1,0:T(8,128)(2,1)} %pad_maximum_fusion.qw_ref, bf16[640,128]{1,0:T(8,128)(2,1)} %pad_maximum_fusion.1.qn_ref, bf16[2,320,512]{2,1,0:T(8,128)(2,1)} %bitcast.10, bf16[2,160,128]{2,1,0:T(8,128)(2,1)} %copy.53.rope_ref, bf16[512,256]{1,0:T(8,128)(2,1)} %ew_ref.1, ...), custom_call_target="tpu_custom_call" | custom-call | tf_op jit(solution)/shard_map/pallas_call | solution.py:571
  174.2 1.7 copy.66
  (14 shorter events, 0.1 us)
Async XLA Ops:
  0.0 1.2 slice-start
  1.1 0.9 copy-start.1
  2.1 1.7 slice-start.1
  4.0 1.7 copy-start
  4.9 1.0 copy-start.4
  7.0 1.0 copy-start.5
  7.0 1.6 slice-start.2
  7.3 1.5 slice-start.4
  8.6 0.7 slice-start.3
  8.6 0.8 slice-start.5
  8.8 1.6 copy-start.2
  9.0 2.3 %copy-start.3 = (f32[3,2,704]{2,1,0:T(2,128)S(1)}, f32[3,2,704]{2,1,0:T(2,128)}, u32[]{:S(2)}) copy-start(f32[3,2,704]{2,1,0:T(2,128)} %param.29) | copy-start | bytes 50692

commit v2 on v1

v2 whole, which is shorter than its diff:
```python
import jax
import jax.numpy as jnp
import numpy as np
from jax import lax
from jax.experimental import pallas as pl
from jax.experimental.pallas import tpu as pltpu
from jax.sharding import PartitionSpec as P

D = 2048
FF = 5632
RANK = 512
ROPE = 64
NOPE_W = 128
VAL_W = 128
NOPE_N = 64
VAL_N = 64
N_TP = 8
N_SP = 16
ROWS = 640
UNITS = FF // N_TP
FEATS = D // N_TP
EDGE = 16

theta = 10000.0
epsilon = 1e-06
LOG2E = 1.4426950408889634
SCALE_W = (NOPE_W + ROPE) ** -0.5 * LOG2E
SCALE_N = (NOPE_N + ROPE) ** -0.5 * LOG2E

MESH = pl.DeviceIdType.MESH
F32 = jnp.float32
BF16 = jnp.bfloat16

ORDER = (
    (0, 0), (1, 0), (3, 0), (0, 1), (0, 3), (2, 0), (1, 1), (1, 3),
    (3, 1), (3, 3), (0, 2), (2, 1), (2, 3), (1, 2), (3, 2), (2, 2),
)
SLOT = {offset: index for index, offset in enumerate(ORDER)}
PAIRS = len(ORDER) // 2
KEYS = 1280
CHUNK = 64
UP_START = 5
DN_START = 7


class Place:
    def __init__(self):
        self.sp = lax.axis_index("sp")
        self.tp = lax.axis_index("tp")
        self.z, self.y = lax.div(self.sp, 4), lax.rem(self.sp, 4)
        self.x, self.c = lax.div(self.tp, 2), lax.rem(self.tp, 2)

    def along(self, first, second):
        z = lax.rem(self.z + first * (1 - self.c) + second * self.c, 4)
        y = lax.rem(self.y + first * self.c + second * (1 - self.c), 4)
        return z * 4 + y

    def device(self, first, second):
        return {"sp": self.along(first, second), "tp": self.tp}

    def feature(self, dx, other=0):
        core = self.c if not other else 1 - self.c
        return lax.rem(self.x + dx, 4) * 2 + core

    def peer(self, dx, other=0):
        return {"sp": self.sp, "tp": self.feature(dx, other)}


class Copies:
    def __init__(self):
        self.sent = []

    def start(self, build):
        def copy():
            src, dst, send, recv, device = build()
            return pltpu.make_async_remote_copy(
                src_ref=src, dst_ref=dst, send_sem=send, recv_sem=recv, device_id=device, device_id_type=MESH
            )

        copy().start()
        self.sent.append(copy)

    def arrived(self, dst, recv, device):
        pltpu.make_async_remote_copy(
            src_ref=dst, dst_ref=dst, send_sem=recv, recv_sem=recv, device_id=device, device_id_type=MESH
        ).wait_recv()

    def drain(self):
        for copy in self.sent:
            copy().wait_send()
        self.sent = []


def onward(offset):
    df, ds = offset
    moves = []
    if ds == 0:
        if df == 3:
            moves.append((1, 0, 0, (2, 0)))
        if df == 1:
            moves.append((3, 0, 1, (2, 0)))
        if df == 0:
            moves.append((1, 0, None, (3, 0)))
            moves.append((3, 0, None, (1, 0)))
        moves.append((0, 1, None, (df, 3)))
        moves.append((0, 3, None, (df, 1)))
    elif ds == 3:
        moves.append((0, 1, 0, (df, 2)))
    elif ds == 1:
        moves.append((0, 3, 1, (df, 2)))
    return moves


MOVES = [(offset, move) for offset in ORDER for move in onward(offset)]
SEND = {key: index for index, key in enumerate(MOVES)}
N_SEND = len(MOVES)


class Gather:
    def __init__(self, copies, place, view, send, recv, own=None):
        self.copies, self.place, self.view = copies, place, view
        self.send, self.recv, self.own = send, recv, own

    def forward(self, offset):
        for move in onward(offset):
            for part in range(self.send.shape[0]):
                self.copies.start(lambda move=move, part=part: self._copy(offset, move, part))

    def _copy(self, offset, move, part):
        first, second, half, target = move
        source = self.own(half) if offset == (0, 0) and self.own else self.view(offset, half)
        return (
            source[part],
            self.landing(offset, target, half)[part],
            self.send.at[part, SEND[(offset, move)]],
            self.recv.at[part, SLOT[target] * 2 + (half or 0)],
            self.place.device(first, second),
        )

    def landing(self, offset, target, half):
        return self.view(target, half)

    def wait(self, offset):
        if offset == (0, 0):
            return
        halves = (0, 1) if 2 in offset and not (offset[0] == 2 and offset[1] in (1, 3)) else (None,)
        for half in halves:
            for part, dst in enumerate(self.view(offset, half)):
                self.copies.arrived(
                    dst, self.recv.at[part, SLOT[offset] * 2 + (half or 0)], self.place.device(0, 1)
                )


class GatherPlaced(Gather):
    def landing(self, offset, target, half):
        return self.view(offset, half)


class RingGather:
    def __init__(self, copies, place, view, send, recv):
        self.copies, self.place, self.view = copies, place, view
        self.send, self.recv = send, recv

    def _send(self, feature, half, index, arrival, device):
        for part, ref in enumerate(self.view(feature, half)):
            self.copies.start(
                lambda part=part, ref=ref: (ref, ref, self.send.at[part, index], self.recv.at[part, arrival], device)
            )

    def _wait(self, feature, half, arrival):
        for part, ref in enumerate(self.view(feature, half)):
            self.copies.arrived(ref, self.recv.at[part, arrival], self.place.peer(0, 1))

    def begin(self):
        place = self.place
        me = place.feature(0)
        self._send(me, None, 0, 0, place.peer(1))
        self._send(me, None, 1, 1, place.peer(3))
        self._send(me, None, 2, 4, place.peer(0, 1))

    def middle(self):
        place = self.place
        left, right = place.feature(3), place.feature(1)
        self._wait(left, None, 0)
        self._send(left, 0, 3, 2, place.peer(1))
        self._send(left, None, 4, 5, place.peer(0, 1))
        self._wait(right, None, 1)
        self._send(right, 1, 5, 3, place.peer(3))
        self._send(right, None, 6, 6, place.peer(0, 1))

    def end(self):
        place = self.place
        far = place.feature(2)
        self._wait(far, 0, 2)
        self._wait(far, 1, 3)
        self._send(far, None, 7, 7, place.peer(0, 1))
        self._wait(place.feature(0, 1), None, 4)
        self._wait(place.feature(3, 1), None, 5)
        self._wait(place.feature(1, 1), None, 6)
        self._wait(place.feature(2, 1), None, 7)


def half_rows(half, rows, start=0):
    if half is None:
        return pl.ds(start, rows)
    return pl.ds(start + half * (rows // 2), rows // 2)


def kernel(
    qw_hbm, qn_hbm, lat_hbm, rope_hbm, lgain_hbm, ew_hbm, en_hbm, res_hbm, ow_ref, on_ref, gain_ref, ug_ref, uv_ref, dn_ref,
    taps_hbm, inv_hbm, out_ref,
    latb, ropb, upf, dnf, kbuf, vbuf, sbuf, pbuf, mrow, acc, hw, hn, oww, ownr, own0, own1, gains, att, nrm, gx, vx, hid,
    part, send_a, recv_a, send_b, recv_b, send_c, recv_c,
    qt, qraw, qw_ref, qn_ref, lraw, rraw, lgain, ew_ref, en_ref, res_ref, taps_ref, inv_ref,
    ls, lr, lps, lpr, us, ur, ds_, dr, hs, hr, as_, ar, xs, xr, es, er, rs, rr, local,
):
    place = Place()
    copies = Copies()
    c, tp, sp = place.c, place.tp, place.sp

    mine = pl.ds(pl.multiple_of(tp * FEATS, FEATS), FEATS)
    loads = [
        (lat_hbm, lraw), (rope_hbm, rraw), (lgain_hbm, lgain), (inv_hbm, inv_ref), (qw_hbm, qt), (qn_hbm, qraw),
        (ew_hbm, ew_ref), (en_hbm, en_ref), (ug_ref, upf.at[sp, 0:UNITS]), (uv_ref, upf.at[sp, UNITS : 2 * UNITS]),
        (dn_ref, dnf.at[sp]), (ow_ref.at[:, mine], oww.at[tp]), (on_ref.at[:, mine], ownr.at[tp]),
        (gain_ref, gains.at[tp]), (res_hbm, res_ref), (taps_hbm, taps_ref),
    ]

    def load(index):
        src, dst = loads[index]
        return pltpu.make_async_copy(src, dst, local.at[index])

    for index in range(len(loads)):
        load(index).start()

    barrier = pltpu.get_barrier_semaphore()
    talk = [place.device(f, s) for f, s in ((1, 0), (3, 0), (0, 1), (0, 3))]
    talk += [{"sp": sp, "tp": lax.rem(tp + d, N_TP)} for d in range(1, N_TP)]
    talk += [{"sp": lax.rem(sp + d, N_SP), "tp": tp} for d in (1, N_SP - 1)]
    for device in talk:
        pl.semaphore_signal(barrier, inc=1, device_id=device, device_id_type=MESH)

    for index in range(4):
        load(index).wait()
    for half in range(2):
        floats = lraw[half * 320 : half * 320 + 320, :].astype(F32)
        mean = jnp.sum(floats * floats, axis=1, keepdims=True) * (1.0 / RANK)
        latb[half, 0] = (floats * lax.rsqrt(mean + epsilon) * lgain[...]).astype(BF16)
    position = (lax.broadcasted_iota(jnp.int32, (32, ROWS), 1) + sp * ROWS).astype(F32)
    angles = position * inv_ref[:, 0:1]
    cosine, sine = jnp.cos(angles), jnp.sin(angles)

    def turn(floats):
        lower, upper = floats[0:32], floats[32:64]
        return [lower * cosine - upper * sine, lower * sine + upper * cosine]

    turned = turn(rraw[...].astype(F32))
    doubled = jnp.transpose(jnp.concatenate(turned + turned, axis=0))
    lane = lax.broadcasted_iota(jnp.int32, (160, 128), 1)
    for half in range(2):
        start = half * 320
        ropb[half, 0] = jnp.where(lane < 64, doubled[start : start + 160], doubled[start + 160 : start + 320]).astype(BF16)

    pl.semaphore_wait(barrier, len(talk))

    lat_gather = Gather(
        copies,
        place,
        lambda offset, half: [
            latb.at[c, SLOT[offset], half_rows(half, 320)],
            ropb.at[c, SLOT[offset], half_rows(half, 160)],
        ],
        ls,
        lr,
    )

    def up_view(offset, half):
        return [upf.at[place.along(*offset), half_rows(half, 2 * UNITS)]]

    def dn_view(offset, half):
        return [dnf.at[place.along(*offset), half_rows(half, UNITS)]]

    up_gather = GatherPlaced(copies, place, up_view, us, ur)
    dn_gather = GatherPlaced(copies, place, dn_view, ds_, dr)

    lat_gather.forward((0, 0))

    def exchange(d, start):
        to, source = lax.rem(tp + d, N_TP), lax.rem(tp + N_TP - d, N_TP)
        theirs = pl.ds(pl.multiple_of(to * FEATS, FEATS), FEATS)
        arrays = (
            (ow_ref.at[:, theirs], oww.at[tp], oww.at[source]),
            (on_ref.at[:, theirs], ownr.at[tp], ownr.at[source]),
            (gain_ref, gains.at[tp], gains.at[source]),
        )
        for index, (src, dst, landed) in enumerate(arrays):
            if start:
                copies.start(
                    lambda src=src, dst=dst, index=index: (
                        src, dst, xs.at[index, d], xr.at[index, d], {"sp": sp, "tp": to}
                    )
                )
            else:
                copies.arrived(landed, xr.at[index, d], {"sp": sp, "tp": to})

    for d in range(1, N_TP):
        exchange(d, True)

    for index in (4, 5):
        load(index).wait()
    blank = jnp.zeros((64, ROWS), F32)
    rope_part = [SCALE_W * piece for piece in turn(qt[128:192, :].astype(F32))]
    qw_ref[:, 0:128] = jnp.transpose(qt[0:128, :].astype(F32)).astype(BF16)
    qw_ref[:, 128:256] = jnp.transpose(jnp.concatenate([blank] + rope_part, axis=0)).astype(BF16)
    narrow_query = jnp.transpose(qraw[...].astype(F32))
    rope_part = [SCALE_N * piece for piece in turn(narrow_query[64:128])]
    qn_ref[...] = jnp.transpose(jnp.concatenate([narrow_query[0:64]] + rope_part, axis=0)).astype(BF16)
    for index in (6, 7):
        load(index).wait()

    mrow[...] = jnp.full_like(mrow, -1e30)
    acc[...] = jnp.zeros_like(acc)

    def partner_view(core, slot):
        return [latb.at[core, slot], ropb.at[core, slot]]

    def own_arrivals(k):
        for slot in (2 * k, 2 * k + 1):
            if slot == 0:
                continue
            lat_gather.wait(ORDER[slot])
            lat_gather.forward(ORDER[slot])
            for index in range(2):
                copies.start(
                    lambda index=index, slot=slot: (
                        partner_view(c, slot)[index], partner_view(c, slot)[index],
                        lps.at[index, slot], lpr.at[index, slot], place.peer(0, 1),
                    )
                )
        if k == UP_START:
            for index in (8, 9):
                load(index).wait()
            up_gather.forward((0, 0))
        if k == DN_START:
            load(10).wait()
            dn_gather.forward((0, 0))

    def partner_arrivals(k):
        for slot in (2 * k, 2 * k + 1):
            if slot:
                for index, ref in enumerate(partner_view(1 - c, slot)):
                    copies.arrived(ref, lpr.at[index, slot], place.peer(0, 1))

    def expand(pair, side):
        lane = lax.broadcasted_iota(jnp.int32, (160, 128), 1)
        for u in range(4):
            block = latb[u % 2, 2 * pair + u // 2]
            rope = ropb[u % 2, 2 * pair + u // 2].astype(F32)
            wide = jnp.dot(block, ew_ref[...], preferred_element_type=F32)
            narrow = jnp.dot(block, en_ref[...], preferred_element_type=F32)
            rows = pl.ds(u * 320, 320)
            kbuf[side, rows, 0:128] = (wide[:, :128] * SCALE_W).astype(BF16)
            vbuf[side, rows, 0:128] = wide[:, 128:].astype(BF16)
            scaled = narrow * SCALE_N
            kbuf[side, pl.ds(u * 320, 160), 128:256] = jnp.where(
                lane < 64, scaled[:160], pltpu.roll(rope, 64, 1)
            ).astype(BF16)
            kbuf[side, pl.ds(u * 320 + 160, 160), 128:256] = jnp.where(lane < 64, scaled[160:], rope).astype(BF16)
            for row in (0, 160):
                vbuf[side, pl.ds(u * 320 + row, 160), 128:256] = jnp.where(lane < 64, 1.0, narrow[row : row + 160]).astype(
                    BF16
                )

    def score(group, side):
        q_ref, lanes = (qw_ref, slice(0, 256)) if group == 0 else (qn_ref, slice(128, 256))
        sbuf[group] = lax.dot_general(
            q_ref[...], kbuf[side, :, lanes], (((1,), (1,)), ((), ())), preferred_element_type=F32
        )

    def soften(group):
        for start in range(0, ROWS, CHUNK):
            rows = slice(start, start + CHUNK)
            kept = slice(group * ROWS + start, group * ROWS + start + CHUNK)
            scores = sbuf[group, rows, :]
            before = mrow[kept, :]
            top = jnp.maximum(before, jnp.max(scores, axis=1, keepdims=True))
            mrow[kept, :] = top
            pbuf[group, rows, :] = jnp.exp2(scores - top[:, 0:1]).astype(BF16)
            shrink = jnp.exp2(before - top)
            acc[kept, 0:128] = shrink * acc[kept, 0:128]
            if group == 0:
                acc[kept, 128:256] = shrink * acc[kept, 128:256]

    def gain_values(group, side):
        if group == 0:
            acc[0:ROWS, :] += jnp.dot(pbuf[0], vbuf[side], preferred_element_type=F32)
        else:
            acc[ROWS : 2 * ROWS, 0:128] += jnp.dot(pbuf[1], vbuf[side, :, 128:256], preferred_element_type=F32)

    own_arrivals(0)
    partner_arrivals(0)
    expand(0, 0)
    score(0, 0)

    def attention_step(pair, carry):
        side = lax.rem(pair, 2)
        for k in range(1, PAIRS):

            @pl.when(pair == k - 1)
            def _():
                own_arrivals(k)

        score(1, side)
        soften(0)
        gain_values(0, side)
        for k in range(1, PAIRS):

            @pl.when(pair == k - 1)
            def _():
                partner_arrivals(k)

        expand(pair + 1, 1 - side)
        score(0, 1 - side)
        soften(1)
        gain_values(1, side)
        return carry

    lax.fori_loop(0, PAIRS - 1, attention_step, 0)
    last = (PAIRS - 1) % 2
    score(1, last)
    soften(0)
    gain_values(0, last)
    soften(1)
    gain_values(1, last)

    hw[tp] = (acc[0:ROWS, 0:128] / acc[0:ROWS, 128:129]).astype(BF16)
    low = acc[ROWS : ROWS + 320, 0:128] / acc[ROWS : ROWS + 320, 0:1]
    high = acc[ROWS + 320 : 2 * ROWS, 0:128] / acc[ROWS + 320 : 2 * ROWS, 0:1]
    lane = lax.broadcasted_iota(jnp.int32, (320, 128), 1)
    hn[tp] = jnp.where(lane < 64, pltpu.roll(low, 64, 1), high).astype(BF16)
    head_gather = RingGather(
        copies,
        place,
        lambda feature, half: [hw.at[feature, half_rows(half, 640)], hn.at[feature, half_rows(half, 320)]],
        hs,
        hr,
    )
    head_gather.begin()

    for offset in ((1, 0), (3, 0), (0, 1), (0, 3)):
        up_gather.wait(offset)
        up_gather.forward(offset)

    for d in range(1, N_TP):
        exchange(d, False)
    for index in range(11, 16):
        load(index).wait()
    zero = jnp.zeros((64, FEATS), BF16)
    for j in range(N_TP):
        own0[pl.ds(j * 128, 64), :] = ownr[j]
        own0[pl.ds(j * 128 + 64, 64), :] = zero
        own1[pl.ds(j * 128, 64), :] = zero
        own1[pl.ds(j * 128 + 64, 64), :] = ownr[j]

    head_gather.middle()
    for offset in ((2, 0), (1, 1), (1, 3), (3, 1), (3, 3)):
        up_gather.wait(offset)
        up_gather.forward(offset)
    for offset in ((1, 0), (3, 0), (0, 1), (0, 3)):
        dn_gather.wait(offset)
        dn_gather.forward(offset)
    head_gather.end()

    wide_heads = jnp.concatenate([hw[j] for j in range(N_TP)], axis=1)
    narrow_heads = jnp.concatenate([hn[j] for j in range(N_TP)], axis=1)
    summed = jnp.dot(wide_heads, oww[...].reshape(N_TP * 128, FEATS), preferred_element_type=F32)
    top = jnp.dot(narrow_heads, own0[...], preferred_element_type=F32)
    bottom = jnp.dot(narrow_heads, own1[...], preferred_element_type=F32)
    att[tp, 0:320] = (res_ref[0:320, :].astype(F32) + summed[0:320] + top).astype(BF16)
    att[tp, 320:640] = (res_ref[320:640, :].astype(F32) + summed[320:640] + bottom).astype(BF16)

    att_gather = RingGather(
        copies, place, lambda feature, half: [att.at[feature, half_rows(half, 640)]], as_, ar
    )
    att_gather.begin()
    for offset in ((0, 2), (2, 1), (2, 3)):
        up_gather.wait(offset)
        up_gather.forward(offset)
    att_gather.middle()
    for offset in ((1, 2), (3, 2), (2, 2)):
        up_gather.wait(offset)
        up_gather.forward(offset)
    for offset in ((2, 0), (1, 1), (1, 3), (3, 1), (3, 3)):
        dn_gather.wait(offset)
        dn_gather.forward(offset)
    att_gather.end()

    def norm_step(index, carry):
        rows = pl.ds(index * 64, 64)
        squares = jnp.zeros((64, FEATS), F32)
        for j in range(N_TP):
            piece = att[j, rows, :].astype(F32)
            squares = squares + piece * piece
        factor = lax.rsqrt(jnp.sum(squares, axis=1, keepdims=True) * (1.0 / D) + epsilon)
        for j in range(N_TP):
            nrm[rows, j * FEATS : (j + 1) * FEATS] = (
                att[j, rows, :].astype(F32) * factor * gains[j]
            ).astype(BF16)
        return carry

    lax.fori_loop(0, ROWS // 64, norm_step, 0)

    for base, dest in ((0, gx), (UNITS, vx)):
        for start in (0, 256, 512):
            stop = min(start + 256, UNITS)
            weights = jnp.concatenate([upf[o, base + start : base + stop, :] for o in range(N_SP)], axis=1)
            dest[EDGE : EDGE + ROWS, start:stop] = lax.dot_general(
                nrm[...], weights, (((1,), (1,)), ((), ())), preferred_element_type=F32
            ).astype(BF16)

    following = {"sp": lax.rem(sp + 1, N_SP), "tp": tp}
    leading = {"sp": lax.rem(sp + N_SP - 1, N_SP), "tp": tp}
    edges = [
        (rows, landing, 2 * index + side, device)
        for side, (rows, landing, device) in enumerate(((ROWS, 0, following), (EDGE, ROWS + EDGE, leading)))
        for index in range(2)
    ]

    def edge(rows, landing, index, device):
        ref = (gx, vx)[index // 2]
        return ref.at[pl.ds(rows, EDGE)], ref.at[pl.ds(landing, EDGE)], es.at[index], er.at[index], device

    for entry in edges:
        copies.start(lambda entry=entry: edge(*entry))
    for offset in ((0, 2), (2, 1), (2, 3)):
        dn_gather.wait(offset)
        dn_gather.forward(offset)
    for rows, landing, index, device in edges:
        copies.arrived(edge(rows, landing, index, device)[1], er.at[index], device)

    def conv_step(index, carry):
        span = pl.ds(index * 128, 160)
        position = lax.broadcasted_iota(jnp.int32, (160, 1), 0) + index * 128 - EDGE
        outside = ((sp == 0) & (position < 0)) | ((sp == N_SP - 1) & (position >= ROWS))

        def smooth(ref, which, columns):
            wide = jnp.where(outside, 0.0, ref[span, columns].astype(F32))
            low = pltpu.roll(wide, 1, 0)[16:144]
            high = pltpu.roll(wide, 159, 0)[16:144]
            taps = [taps_ref[k, which : which + 1, columns] for k in range(3)]
            return taps[0] * low + taps[1] * wide[16:144] + taps[2] * high

        rows = pl.ds(index * 128, 128)
        for start in range(0, UNITS, 128):
            columns = slice(start, min(start + 128, UNITS))
            gate = smooth(gx, 0, columns)
            value = smooth(vx, 1, columns)
            hid[rows, columns] = (gate / (1.0 + jnp.exp(-gate)) * value).astype(BF16)
        return carry

    lax.fori_loop(0, 5, conv_step, 0)

    for offset in ((1, 2), (3, 2), (2, 2)):
        dn_gather.wait(offset)
        dn_gather.forward(offset)

    def down(feature):
        weights = jnp.concatenate([dnf[2 * feature], dnf[2 * feature + 1]], axis=1)
        return jnp.dot(hid[...], weights, preferred_element_type=F32)

    def down_pair(dx):
        send_a[dx] = down(place.feature(dx, 1)).astype(BF16)
        copies.start(lambda: (send_a.at[dx], recv_a.at[dx], rs.at[dx], rr.at[dx], place.peer(0, 1)))
        part[dx] = down(place.feature(dx))

    def pair_sum(dx):
        copies.arrived(recv_a.at[dx], rr.at[dx], place.peer(0, 1))
        return part[dx] + recv_a[dx].astype(F32)

    def send_half(side, index, dx):
        rows = pl.ds(320 * (index % 2), 320)
        copies.start(
            lambda: (send_c.at[side, rows], recv_c.at[side, rows], rs.at[6 + index], rr.at[6 + index], place.peer(dx))
        )

    down_pair(2)
    down_pair(1)
    far = pair_sum(2)
    send_b[0] = far[0:320].astype(BF16)
    copies.start(lambda: (send_b.at[0], recv_b.at[0], rs.at[4], rr.at[4], place.peer(1)))
    send_b[1] = far[320:640].astype(BF16)
    copies.start(lambda: (send_b.at[1], recv_b.at[1], rs.at[5], rr.at[5], place.peer(3)))
    down_pair(3)
    right = pair_sum(1)
    send_c[0, 320:640] = right[320:640].astype(BF16)
    send_half(0, 1, 1)
    part[1, 0:320] = right[0:320]
    down_pair(0)
    left = pair_sum(3)
    send_c[1, 0:320] = left[0:320].astype(BF16)
    send_half(1, 2, 3)
    copies.arrived(recv_b.at[0], rr.at[4], place.peer(1))
    send_c[0, 0:320] = (part[1, 0:320] + recv_b[0].astype(F32)).astype(BF16)
    send_half(0, 0, 1)
    copies.arrived(recv_b.at[1], rr.at[5], place.peer(3))
    send_c[1, 320:640] = (left[320:640] + recv_b[1].astype(F32)).astype(BF16)
    send_half(1, 3, 3)
    own_sum = pair_sum(0) + att[tp].astype(F32)
    for side, index in ((0, 1), (1, 2), (0, 0), (1, 3)):
        copies.arrived(recv_c.at[side, pl.ds(320 * (index % 2), 320)], rr.at[6 + index], place.peer(1))
    out_ref[...] = (own_sum + recv_c[0].astype(F32) + recv_c[1].astype(F32)).astype(BF16)
    copies.drain()


def per_device(
    residual, query_wide, query_narrow, latent, rope_key, latent_gain, expand_wide, expand_narrow,
    out_wide, out_narrow, norm_gain, up_gate, up_value, down_weight, conv_taps,
):
    inverse = np.power(np.float32(theta), -2.0 * np.arange(32, dtype=np.float32) / ROPE).astype(np.float32)
    inverse = jnp.asarray(np.broadcast_to(inverse[:, None], (32, 128)))
    vmem = pl.BlockSpec(memory_space=pltpu.VMEM)
    anywhere = pl.BlockSpec(memory_space=pl.ANY)
    dma = pltpu.SemaphoreType.DMA
    return pl.pallas_call(
        kernel,
        out_shape=jax.ShapeDtypeStruct((ROWS, FEATS), BF16),
        in_specs=[anywhere] * 16,
        out_specs=vmem,
        scratch_shapes=[
            pltpu.VMEM((2, 16, 320, RANK), BF16),
            pltpu.VMEM((2, 16, 160, 128), BF16),
            pltpu.VMEM((N_SP, 2 * UNITS, 128), BF16),
            pltpu.VMEM((N_SP, UNITS, 128), BF16),
            pltpu.VMEM((2, KEYS, 256), BF16),
            pltpu.VMEM((2, KEYS, 256), BF16),
            pltpu.VMEM((2, ROWS, KEYS), F32),
            pltpu.VMEM((2, ROWS, KEYS), BF16),
            pltpu.VMEM((2 * ROWS, 128), F32),
            pltpu.VMEM((2 * ROWS, 256), F32),
            pltpu.VMEM((N_TP, ROWS, 128), BF16),
            pltpu.VMEM((N_TP, ROWS // 2, 128), BF16),
            pltpu.VMEM((N_TP, 128, FEATS), BF16),
            pltpu.VMEM((N_TP, 64, FEATS), BF16),
            pltpu.VMEM((N_TP * 128, FEATS), BF16),
            pltpu.VMEM((N_TP * 128, FEATS), BF16),
            pltpu.VMEM((N_TP, 1, FEATS), F32),
            pltpu.VMEM((N_TP, ROWS, FEATS), BF16),
            pltpu.VMEM((ROWS, D), BF16),
            pltpu.VMEM((ROWS + 2 * EDGE, UNITS), BF16),
            pltpu.VMEM((ROWS + 2 * EDGE, UNITS), BF16),
            pltpu.VMEM((ROWS, UNITS), BF16),
            pltpu.VMEM((4, ROWS, FEATS), F32),
            pltpu.VMEM((4, ROWS, FEATS), BF16),
            pltpu.VMEM((4, ROWS, FEATS), BF16),
            pltpu.VMEM((2, ROWS // 2, FEATS), BF16),
            pltpu.VMEM((2, ROWS // 2, FEATS), BF16),
            pltpu.VMEM((2, ROWS, FEATS), BF16),
            pltpu.VMEM((2, ROWS, FEATS), BF16),
            pltpu.VMEM((NOPE_W + ROPE, ROWS), BF16),
            pltpu.VMEM((ROWS, 128), BF16),
            pltpu.VMEM((ROWS, 256), BF16),
            pltpu.VMEM((ROWS, 128), BF16),
            pltpu.VMEM((ROWS, RANK), BF16),
            pltpu.VMEM((ROPE, ROWS), BF16),
            pltpu.VMEM((1, RANK), F32),
            pltpu.VMEM((RANK, 256), BF16),
            pltpu.VMEM((RANK, 128), BF16),
            pltpu.VMEM((ROWS, FEATS), BF16),
            pltpu.VMEM((3, 2, UNITS), F32),
            pltpu.VMEM((32, 128), F32),
            dma((2, N_SEND)), dma((2, 32)), dma((2, 16)), dma((2, 16)),
            dma((1, N_SEND)), dma((1, 32)),
            dma((1, N_SEND)), dma((1, 32)),
            dma((2, 8)), dma((2, 8)),
            dma((1, 8)), dma((1, 8)),
            dma((3, 8)), dma((3, 8)),
            dma((4,)), dma((4,)),
            dma((10,)), dma((10,)),
            dma((16,)),
        ],
        compiler_params=pltpu.CompilerParams(
            collective_id=0, has_side_effects=True, vmem_limit_bytes=67043328
        ),
    )(
        query_wide.T, query_narrow, latent, rope_key.T, latent_gain.reshape(1, RANK), expand_wide, expand_narrow,
        residual, out_wide, out_narrow, norm_gain.reshape(1, FEATS), up_gate.T, up_value.T, down_weight.T, conv_taps, inverse,
    )


def solution(mesh):
    in_specs = (
        P("sp", "tp"), P("sp", "tp"), P("sp", "tp"), P("sp", None), P("sp", None), P(),
        P(None, "tp"), P(None, "tp"), P("tp", None), P("tp", None), P("tp"),
        P("sp", "tp"), P("sp", "tp"), P("sp", "tp"), P(None, None, "tp"),
    )
    return jax.shard_map(
        per_device, mesh=mesh, in_specs=in_specs, out_specs=P("sp", "tp"), check_vma=False
    )
```

time: 176 us -> 127 us (0.72)
  Pallas kernels: 162 us -> 124 us
  local copies, waits for them, and re-layouts: 8.72 us -> 3.05 us
  other arithmetic: 4.84 us -> 0 us
    pallas_call x1, Pallas kernels: 162 us -> 124 us  [per_device(): pl.pallas_call(kernel, out_shape=jax.ShapeDtypeStruct((ROWS, FEATS), BF16...]
    unnamed x21 -> x3, local copies, waits for them, and re-layouts: 5.17 us -> 2.37 us
    concatenate x5 -> x0, local copies, waits for them, and re-layouts: 1.81 us -> none  [the longest x2 1.56 us: interleave(): jnp.concatenate([gate[:, :640], value[:, :640], gate[:, 640:], value[:, 6...]
where the time goes in v2:
time: 127 us
  Pallas kernels  124 us (98%)
  local copies, waits for them, and re-layouts  3.05 us (2%)
    pallas_call x1, Pallas kernels, per_device(): pl.pallas_call(kernel, out_shape=jax.ShapeDtypeStruct((ROWS, FEATS), BF16...  124 us

profile of v2, /device:TPU:1, one launch (start us, length us, event | category | flops | bytes accessed | tf_op | source)
XLA Modules:
  0.0 126.7 jit_solution(1423540523953961643)
XLA Ops:
  0.0 0.0 copy-start
  0.0 0.7 copy-done
  0.7 0.7 jit_solution_.3.inv_hbm
  1.3 123.6 %shard_map.154 = bf16[640,256]{1,0:T(8,128)(2,1)} custom-call(bf16[192,640]{1,0:T(8,128)(2,1)} %bitcast.7, bf16[640,128]{1,0:T(8,128)(2,1)} %qn_hbm.1, bf16[640,512]{1,0:T(8,128)(2,1)} %lat_hbm.1, bf16[64,640]{1,0:T(8,128)(2,1)} %bitcast.11, f32[1,512]{1,0:T(1,128)} %bitcast.12, bf16[512,256]{1,0:T(8,128)(2,1)} %ew_hbm.1, bf16[512,128]{1,0:T(8,128)(2,1)} %en_hbm.1, ...), custom_call_target="tpu_custom_call" | custom-call | tf_op jit(solution)/shard_map/pallas_call | solution.py:624
  124.9 1.7 %copy.18 = bf16[640,256]{1,0:T(8,128)(2,1)} copy(bf16[640,256]{1,0:T(8,128)(2,1)} %shard_map.154) | data formatting | bytes 655360
Async XLA Ops:
  0.0 0.7 copy-start

commit v3 on v2

--- a/solution.py
+++ b/solution.py
@@ -32,15 +32,30 @@
 BF16 = jnp.bfloat16
 
 ORDER = (
-    (0, 0), (1, 0), (3, 0), (0, 1), (0, 3), (2, 0), (1, 1), (1, 3),
-    (3, 1), (3, 3), (0, 2), (2, 1), (2, 3), (1, 2), (3, 2), (2, 2),
+    (0, 0), (1, 0), (3, 0), (2, 0), (0, 1), (0, 3), (3, 1), (3, 3),
+    (1, 1), (1, 3), (0, 2), (2, 1), (2, 3), (1, 2), (3, 2), (2, 2),
 )
 SLOT = {offset: index for index, offset in enumerate(ORDER)}
 PAIRS = len(ORDER) // 2
 KEYS = 1280
 CHUNK = 64
-UP_START = 5
-DN_START = 7
+PLANE = 192
+SCHEDULE = {
+    "s0": "E3 E4", "m0": "E6 P1", "s1": "E5 X2", "m1": "E7 X3 P2", "s2": "E8", "m2": "E9 X4 P3", "s3": "E10", "m3": "X5 P4",
+    "m4": "X6 P5", "m5": "X7 P6", "m6": "P7",
+}
+TAKEN = {
+    "E3": ((0, 1), (0, 3)), "E4": ((2, 0),), "E5": ((1, 1), (1, 3)), "E6": ((3, 1), (3, 3)), "E7": ((2, 1), (2, 3)),
+    "E8": ((0, 2),), "E9": ((1, 2), (3, 2)), "E10": ((2, 2),),
+}
+PLAN = {"s2": "U0", "s5": "U1", "heads": "U2 D0", "ended": "U3 D1", "joined": "U4 D2", "up": "D3", "conv": "D4"}
+STEPS = (
+    ((0, 0),),
+    ((1, 0), (3, 0), (0, 1), (0, 3)),
+    ((2, 0), (1, 1), (1, 3), (3, 1), (3, 3)),
+    ((0, 2), (2, 1), (2, 3)),
+    ((1, 2), (3, 2), (2, 2)),
+)
 
 
 class Place:
@@ -100,8 +115,10 @@
         if df == 1:
             moves.append((3, 0, 1, (2, 0)))
         if df == 0:
-            moves.append((1, 0, None, (3, 0)))
-            moves.append((3, 0, None, (1, 0)))
+            moves.append((1, 0, 0, (3, 0)))
+            moves.append((3, 0, 1, (1, 0)))
+            moves.append((1, 0, 1, (3, 0)))
+            moves.append((3, 0, 0, (1, 0)))
         moves.append((0, 1, None, (df, 3)))
         moves.append((0, 3, None, (df, 1)))
     elif ds == 3:
@@ -117,20 +134,19 @@
 
 
 class Gather:
-    def __init__(self, copies, place, view, send, recv, own=None):
+    def __init__(self, copies, place, view, send, recv):
         self.copies, self.place, self.view = copies, place, view
-        self.send, self.recv, self.own = send, recv, own
-
-    def forward(self, offset):
-        for move in onward(offset):
+        self.send, self.recv = send, recv
+
+    def forward(self, offset, only=lambda move: True):
+        for move in filter(only, onward(offset)):
             for part in range(self.send.shape[0]):
                 self.copies.start(lambda move=move, part=part: self._copy(offset, move, part))
 
     def _copy(self, offset, move, part):
         first, second, half, target = move
-        source = self.own(half) if offset == (0, 0) and self.own else self.view(offset, half)
         return (
-            source[part],
+            self.view(offset, half, target)[part],
             self.landing(offset, target, half)[part],
             self.send.at[part, SEND[(offset, move)]],
             self.recv.at[part, SLOT[target] * 2 + (half or 0)],
@@ -138,14 +154,15 @@
         )
 
     def landing(self, offset, target, half):
-        return self.view(target, half)
-
-    def wait(self, offset):
+        return self.view(target, half, target)
+
+    def wait(self, offset, halves=None):
         if offset == (0, 0):
             return
-        halves = (0, 1) if 2 in offset and not (offset[0] == 2 and offset[1] in (1, 3)) else (None,)
+        if halves is None:
+            halves = (0, 1) if offset[1] in (0, 2) else (None,)
         for half in halves:
-            for part, dst in enumerate(self.view(offset, half)):
+            for part, dst in enumerate(self.view(offset, half, offset)):
                 self.copies.arrived(
                     dst, self.recv.at[part, SLOT[offset] * 2 + (half or 0)], self.place.device(0, 1)
                 )
@@ -153,7 +170,7 @@
 
 class GatherPlaced(Gather):
     def landing(self, offset, target, half):
-        return self.view(offset, half)
+        return self.view(offset, half, target)
 
 
 class RingGather:
@@ -161,8 +178,10 @@
         self.copies, self.place, self.view = copies, place, view
         self.send, self.recv = send, recv
 
-    def _send(self, feature, half, index, arrival, device):
+    def _send(self, feature, half, index, arrival, device, parts=None):
         for part, ref in enumerate(self.view(feature, half)):
+            if parts is not None and part not in parts:
+                continue
             self.copies.start(
                 lambda part=part, ref=ref: (ref, ref, self.send.at[part, index], self.recv.at[part, arrival], device)
             )
@@ -171,33 +190,37 @@
         for part, ref in enumerate(self.view(feature, half)):
             self.copies.arrived(ref, self.recv.at[part, arrival], self.place.peer(0, 1))
 
-    def begin(self):
+    def begin(self, parts=None):
         place = self.place
         me = place.feature(0)
-        self._send(me, None, 0, 0, place.peer(1))
-        self._send(me, None, 1, 1, place.peer(3))
-        self._send(me, None, 2, 4, place.peer(0, 1))
+        self._send(me, 0, 0, 0, place.peer(1), parts)
+        self._send(me, 1, 1, 3, place.peer(3), parts)
+        self._send(me, 1, 2, 1, place.peer(1), parts)
+        self._send(me, 0, 3, 2, place.peer(3), parts)
+        self._send(me, None, 4, 6, place.peer(0, 1), parts)
 
     def middle(self):
         place = self.place
         left, right = place.feature(3), place.feature(1)
-        self._wait(left, None, 0)
-        self._send(left, 0, 3, 2, place.peer(1))
-        self._send(left, None, 4, 5, place.peer(0, 1))
-        self._wait(right, None, 1)
-        self._send(right, 1, 5, 3, place.peer(3))
-        self._send(right, None, 6, 6, place.peer(0, 1))
+        self._wait(left, 0, 0)
+        self._send(left, 0, 5, 4, place.peer(1))
+        self._wait(right, 1, 3)
+        self._send(right, 1, 6, 5, place.peer(3))
+        self._wait(left, 1, 1)
+        self._send(left, None, 7, 7, place.peer(0, 1))
+        self._wait(right, 0, 2)
+        self._send(right, None, 8, 8, place.peer(0, 1))
 
     def end(self):
         place = self.place
         far = place.feature(2)
-        self._wait(far, 0, 2)
-        self._wait(far, 1, 3)
-        self._send(far, None, 7, 7, place.peer(0, 1))
-        self._wait(place.feature(0, 1), None, 4)
-        self._wait(place.feature(3, 1), None, 5)
-        self._wait(place.feature(1, 1), None, 6)
-        self._wait(place.feature(2, 1), None, 7)
+        self._wait(far, 0, 4)
+        self._wait(far, 1, 5)
+        self._send(far, None, 9, 9, place.peer(0, 1))
+        self._wait(place.feature(0, 1), None, 6)
+        self._wait(place.feature(3, 1), None, 7)
+        self._wait(place.feature(1, 1), None, 8)
+        self._wait(place.feature(2, 1), None, 9)
 
 
 def half_rows(half, rows, start=0):
@@ -212,7 +235,7 @@
     latb, ropb, upf, dnf, kbuf, vbuf, sbuf, pbuf, mrow, acc, hw, hn, oww, ownr, own0, own1, gains, att, nrm, gx, vx, hid,
     part, send_a, recv_a, send_b, recv_b, send_c, recv_c,
     qt, qraw, qw_ref, qn_ref, lraw, rraw, lgain, ew_ref, en_ref, res_ref, taps_ref, inv_ref,
-    ls, lr, lps, lpr, us, ur, ds_, dr, hs, hr, as_, ar, xs, xr, es, er, rs, rr, local,
+    ls, lr, xls, xlr, lps, lpr, us, ur, ds_, dr, hs, hr, as_, ar, xs, xr, es, er, rs, rr, local,
 ):
     place = Place()
     copies = Copies()
@@ -263,27 +286,35 @@
 
     pl.semaphore_wait(barrier, len(talk))
 
-    lat_gather = Gather(
-        copies,
-        place,
-        lambda offset, half: [
-            latb.at[c, SLOT[offset], half_rows(half, 320)],
-            ropb.at[c, SLOT[offset], half_rows(half, 160)],
-        ],
-        ls,
-        lr,
-    )
-
-    def up_view(offset, half):
+    def lat_rows(half, target):
+        if target[1] == 0:
+            return half_rows(half, 320)
+        start = lax.rem(place.x, 2) * (320 - PLANE)
+        if half is None:
+            return pl.ds(pl.multiple_of(start, 16), PLANE)
+        return pl.ds(pl.multiple_of(start + half * (PLANE // 2), 16), PLANE // 2)
+
+    def lat_view(offset, half, target):
+        slot = SLOT[offset]
+        return [latb.at[c, slot, lat_rows(half, target)], ropb.at[c, slot, half_rows(half, 160)]]
+
+    def side_rows(slot, index, sent):
+        parity = lax.rem(place.x + (0 if sent else 1), 2)
+        start = parity * PLANE + index * (160 - PLANE // 2)
+        return latb.at[c, slot, pl.ds(pl.multiple_of(start, 16), 160 - PLANE // 2)]
+
+    lat_gather = Gather(copies, place, lat_view, ls, lr)
+
+    def up_view(offset, half, target):
         return [upf.at[place.along(*offset), half_rows(half, 2 * UNITS)]]
 
-    def dn_view(offset, half):
+    def dn_view(offset, half, target):
         return [dnf.at[place.along(*offset), half_rows(half, UNITS)]]
 
     up_gather = GatherPlaced(copies, place, up_view, us, ur)
     dn_gather = GatherPlaced(copies, place, dn_view, ds_, dr)
 
-    lat_gather.forward((0, 0))
+    lat_gather.forward((0, 0), lambda move: move[3][1] == 0)
 
     def exchange(d, start):
         to, source = lax.rem(tp + d, N_TP), lax.rem(tp + N_TP - d, N_TP)
@@ -324,32 +355,62 @@
     def partner_view(core, slot):
         return [latb.at[core, slot], ropb.at[core, slot]]
 
-    def own_arrivals(k):
-        for slot in (2 * k, 2 * k + 1):
-            if slot == 0:
-                continue
-            lat_gather.wait(ORDER[slot])
-            lat_gather.forward(ORDER[slot])
-            for index in range(2):
-                copies.start(
-                    lambda index=index, slot=slot: (
-                        partner_view(c, slot)[index], partner_view(c, slot)[index],
-                        lps.at[index, slot], lpr.at[index, slot], place.peer(0, 1),
-                    )
+    def weights_at(point):
+        for name in PLAN.get(point, "").split():
+            gather, step = (up_gather, dn_gather)[name[0] == "D"], int(name[1])
+            if step == 0:
+                for index in (8, 9) if name[0] == "U" else (10,):
+                    load(index).wait()
+            for offset in STEPS[step]:
+                gather.wait(offset)
+                gather.forward(offset)
+
+    def across(offset):
+        slot = SLOT[offset]
+        for index in range(2):
+            copies.start(
+                lambda index=index: (
+                    partner_view(c, slot)[index], partner_view(c, slot)[index],
+                    lps.at[index, slot], lpr.at[index, slot], place.peer(0, 1),
                 )
-        if k == UP_START:
-            for index in (8, 9):
-                load(index).wait()
-            up_gather.forward((0, 0))
-        if k == DN_START:
-            load(10).wait()
-            dn_gather.forward((0, 0))
-
-    def partner_arrivals(k):
-        for slot in (2 * k, 2 * k + 1):
-            if slot:
-                for index, ref in enumerate(partner_view(1 - c, slot)):
-                    copies.arrived(ref, lpr.at[index, slot], place.peer(0, 1))
+            )
+
+    def plane_arrival(offset):
+        slot = SLOT[offset]
+        lat_gather.wait(offset)
+        lat_gather.forward(offset)
+        if offset[1] == 0:
+            across(offset)
+            return
+        for index, dx in enumerate((1, 3)):
+            copies.start(
+                lambda index=index, dx=dx: (
+                    side_rows(slot, index, True), side_rows(slot, index, True),
+                    xls.at[index, slot], xlr.at[index, slot], place.peer(dx),
+                )
+            )
+
+    def side_arrival(offset):
+        slot = SLOT[offset]
+        for index in range(2):
+            copies.arrived(side_rows(slot, index, False), xlr.at[index, slot], place.peer(1))
+        across(offset)
+
+    def partner_arrival(offset):
+        slot = SLOT[offset]
+        for index, ref in enumerate(partner_view(1 - c, slot)):
+            copies.arrived(ref, lpr.at[index, slot], place.peer(0, 1))
+
+    def take(point):
+        for name in SCHEDULE.get(point, "").split():
+            pair = int(name[1:])
+            if name[0] == "E":
+                for offset in TAKEN[name]:
+                    plane_arrival(offset)
+            else:
+                for offset in ORDER[2 * pair : 2 * pair + 2]:
+                    (side_arrival if name[0] == "X" else partner_arrival)(offset)
+        weights_at(point)
 
     def expand(pair, side):
         lane = lax.broadcasted_iota(jnp.int32, (160, 128), 1)
@@ -397,47 +458,51 @@
         else:
             acc[ROWS : 2 * ROWS, 0:128] += jnp.dot(pbuf[1], vbuf[side, :, 128:256], preferred_element_type=F32)
 
-    own_arrivals(0)
-    partner_arrivals(0)
+    pbuf[1] = jnp.zeros_like(pbuf[1])
+    vbuf[1] = jnp.zeros_like(vbuf[1])
+    for offset, half in (((3, 0), 0), ((1, 0), 1)):
+        lat_gather.wait(offset, (half,))
+        lat_gather.forward(offset, lambda move: move[3] == (2, 0))
+    lat_gather.forward((0, 0), lambda move: move[3][1] != 0)
+    for offset, half in (((1, 0), 0), ((3, 0), 1)):
+        lat_gather.wait(offset, (half,))
+        lat_gather.forward(offset, lambda move: move[3] != (2, 0))
+        across(offset)
+    partner_arrival((1, 0))
     expand(0, 0)
     score(0, 0)
 
     def attention_step(pair, carry):
         side = lax.rem(pair, 2)
-        for k in range(1, PAIRS):
-
-            @pl.when(pair == k - 1)
+        for k in range(PAIRS - 1):
+
+            @pl.when(pair == k)
             def _():
-                own_arrivals(k)
+                take(f"s{k}")
 
         score(1, side)
+        gain_values(1, 1 - side)
         soften(0)
+        for k in range(PAIRS - 1):
+
+            @pl.when(pair == k)
+            def _():
+                take(f"m{k}")
+
+        expand(pair + 1, 1 - side)
         gain_values(0, side)
-        for k in range(1, PAIRS):
-
-            @pl.when(pair == k - 1)
-            def _():
-                partner_arrivals(k)
-
-        expand(pair + 1, 1 - side)
         score(0, 1 - side)
         soften(1)
-        gain_values(1, side)
         return carry
 
     lax.fori_loop(0, PAIRS - 1, attention_step, 0)
+    weights_at("last")
     last = (PAIRS - 1) % 2
     score(1, last)
+    gain_values(1, 1 - last)
     soften(0)
     gain_values(0, last)
-    soften(1)
-    gain_values(1, last)
-
     hw[tp] = (acc[0:ROWS, 0:128] / acc[0:ROWS, 128:129]).astype(BF16)
-    low = acc[ROWS : ROWS + 320, 0:128] / acc[ROWS : ROWS + 320, 0:1]
-    high = acc[ROWS + 320 : 2 * ROWS, 0:128] / acc[ROWS + 320 : 2 * ROWS, 0:1]
-    lane = lax.broadcasted_iota(jnp.int32, (320, 128), 1)
-    hn[tp] = jnp.where(lane < 64, pltpu.roll(low, 64, 1), high).astype(BF16)
     head_gather = RingGather(
         copies,
         place,
@@ -445,11 +510,17 @@
         hs,
         hr,
     )
-    head_gather.begin()
-
-    for offset in ((1, 0), (3, 0), (0, 1), (0, 3)):
-        up_gather.wait(offset)
-        up_gather.forward(offset)
+    head_gather.begin((0,))
+    soften(1)
+    gain_values(1, last)
+
+    low = acc[ROWS : ROWS + 320, 0:128] / acc[ROWS : ROWS + 320, 0:1]
+    high = acc[ROWS + 320 : 2 * ROWS, 0:128] / acc[ROWS + 320 : 2 * ROWS, 0:1]
+    lane = lax.broadcasted_iota(jnp.int32, (320, 128), 1)
+    hn[tp] = jnp.where(lane < 64, pltpu.roll(low, 64, 1), high).astype(BF16)
+    head_gather.begin((1,))
+
+    weights_at("heads")
 
     for d in range(1, N_TP):
         exchange(d, False)
@@ -463,13 +534,9 @@
         own1[pl.ds(j * 128 + 64, 64), :] = ownr[j]
 
     head_gather.middle()
-    for offset in ((2, 0), (1, 1), (1, 3), (3, 1), (3, 3)):
-        up_gather.wait(offset)
-        up_gather.forward(offset)
-    for offset in ((1, 0), (3, 0), (0, 1), (0, 3)):
-        dn_gather.wait(offset)
-        dn_gather.forward(offset)
+    weights_at("middle")
     head_gather.end()
+    weights_at("ended")
 
     wide_heads = jnp.concatenate([hw[j] for j in range(N_TP)], axis=1)
     narrow_heads = jnp.concatenate([hn[j] for j in range(N_TP)], axis=1)
@@ -483,17 +550,11 @@
         copies, place, lambda feature, half: [att.at[feature, half_rows(half, 640)]], as_, ar
     )
     att_gather.begin()
-    for offset in ((0, 2), (2, 1), (2, 3)):
-        up_gather.wait(offset)
-        up_gather.forward(offset)
+    weights_at("begin")
     att_gather.middle()
-    for offset in ((1, 2), (3, 2), (2, 2)):
-        up_gather.wait(offset)
-        up_gather.forward(offset)
-    for offset in ((2, 0), (1, 1), (1, 3), (3, 1), (3, 3)):
-        dn_gather.wait(offset)
-        dn_gather.forward(offset)
+    weights_at("joined")
     att_gather.end()
+    weights_at("full")
 
     def norm_step(index, carry):
         rows = pl.ds(index * 64, 64)
@@ -518,6 +579,7 @@
                 nrm[...], weights, (((1,), (1,)), ((), ())), preferred_element_type=F32
             ).astype(BF16)
 
+    weights_at("up")
     following = {"sp": lax.rem(sp + 1, N_SP), "tp": tp}
     leading = {"sp": lax.rem(sp + N_SP - 1, N_SP), "tp": tp}
     edges = [
@@ -532,9 +594,7 @@
 
     for entry in edges:
         copies.start(lambda entry=entry: edge(*entry))
-    for offset in ((0, 2), (2, 1), (2, 3)):
-        dn_gather.wait(offset)
-        dn_gather.forward(offset)
+    weights_at("edge")
     for rows, landing, index, device in edges:
         copies.arrived(edge(rows, landing, index, device)[1], er.at[index], device)
 
@@ -560,10 +620,7 @@
 
     lax.fori_loop(0, 5, conv_step, 0)
 
-    for offset in ((1, 2), (3, 2), (2, 2)):
-        dn_gather.wait(offset)
-        dn_gather.forward(offset)
-
+    weights_at("conv")
     def down(feature):
         weights = jnp.concatenate([dnf[2 * feature], dnf[2 * feature + 1]], axis=1)
         return jnp.dot(hid[...], weights, preferred_element_type=F32)
@@ -668,11 +725,11 @@
             pltpu.VMEM((ROWS, FEATS), BF16),
             pltpu.VMEM((3, 2, UNITS), F32),
             pltpu.VMEM((32, 128), F32),
-            dma((2, N_SEND)), dma((2, 32)), dma((2, 16)), dma((2, 16)),
+            dma((2, N_SEND)), dma((2, 32)), dma((2, 16)), dma((2, 16)), dma((2, 16)), dma((2, 16)),
             dma((1, N_SEND)), dma((1, 32)),
             dma((1, N_SEND)), dma((1, 32)),
-            dma((2, 8)), dma((2, 8)),
-            dma((1, 8)), dma((1, 8)),
+            dma((2, 10)), dma((2, 10)),
+            dma((1, 10)), dma((1, 10)),
             dma((3, 8)), dma((3, 8)),
             dma((4,)), dma((4,)),
             dma((10,)), dma((10,)),

time: 127 us -> 121 us (0.953)
  Pallas kernels: 124 us -> 118 us
    pallas_call x1, Pallas kernels: 124 us -> 118 us  [per_device(): pl.pallas_call(kernel, out_shape=jax.ShapeDtypeStruct((ROWS, FEATS), BF16...]
where the time goes in v3:
time: 121 us
  Pallas kernels  118 us (98%)
  local copies, waits for them, and re-layouts  3.05 us (3%)
    pallas_call x1, Pallas kernels, per_device(): pl.pallas_call(kernel, out_shape=jax.ShapeDtypeStruct((ROWS, FEATS), BF16...  118 us

profile of v3, /device:TPU:1, one launch (start us, length us, event | category | flops | bytes accessed | tf_op | source)
XLA Modules:
  0.0 120.8 jit_solution(17707585478933886288)
XLA Ops:
  0.0 0.0 copy-start
  0.0 0.7 copy-done
  0.7 0.7 jit_solution_.3.inv_hbm
  1.3 117.8 %shard_map.154 = bf16[640,256]{1,0:T(8,128)(2,1)} custom-call(bf16[192,640]{1,0:T(8,128)(2,1)} %bitcast.7, bf16[640,128]{1,0:T(8,128)(2,1)} %qn_hbm.1, bf16[640,512]{1,0:T(8,128)(2,1)} %lat_hbm.1, bf16[64,640]{1,0:T(8,128)(2,1)} %bitcast.11, f32[1,512]{1,0:T(1,128)} %bitcast.12, bf16[512,256]{1,0:T(8,128)(2,1)} %ew_hbm.1, bf16[512,128]{1,0:T(8,128)(2,1)} %en_hbm.1, ...), custom_call_target="tpu_custom_call" | custom-call | tf_op jit(solution)/shard_map/pallas_call | solution.py:681
  119.1 1.7 %copy.18 = bf16[640,256]{1,0:T(8,128)(2,1)} copy(bf16[640,256]{1,0:T(8,128)(2,1)} %shard_map.154) | data formatting | bytes 655360
Async XLA Ops:
  0.0 0.7 copy-start

commit v4 on v3

--- a/solution.py
+++ b/solution.py
@@ -48,7 +48,9 @@
     "E3": ((0, 1), (0, 3)), "E4": ((2, 0),), "E5": ((1, 1), (1, 3)), "E6": ((3, 1), (3, 3)), "E7": ((2, 1), (2, 3)),
     "E8": ((0, 2),), "E9": ((1, 2), (3, 2)), "E10": ((2, 2),),
 }
-PLAN = {"s2": "U0", "s5": "U1", "heads": "U2 D0", "ended": "U3 D1", "joined": "U4 D2", "up": "D3", "conv": "D4"}
+PLAN = {
+    "s2": "U0", "s5": "U1", "heads": "U2 D0", "begin": "U3 D1", "joined": "U4 D2", "full": "D3", "edge": "D4",
+}
 STEPS = (
     ((0, 0),),
     ((1, 0), (3, 0), (0, 1), (0, 3)),
@@ -595,10 +597,8 @@
     for entry in edges:
         copies.start(lambda entry=entry: edge(*entry))
     weights_at("edge")
-    for rows, landing, index, device in edges:
-        copies.arrived(edge(rows, landing, index, device)[1], er.at[index], device)
-
-    def conv_step(index, carry):
+
+    def conv_step(index, place_of):
         span = pl.ds(index * 128, 160)
         position = lax.broadcasted_iota(jnp.int32, (160, 1), 0) + index * 128 - EDGE
         outside = ((sp == 0) & (position < 0)) | ((sp == N_SP - 1) & (position >= ROWS))
@@ -610,62 +610,105 @@
             taps = [taps_ref[k, which : which + 1, columns] for k in range(3)]
             return taps[0] * low + taps[1] * wide[16:144] + taps[2] * high
 
-        rows = pl.ds(index * 128, 128)
+        rows = pl.ds(place_of * 128, 128)
         for start in range(0, UNITS, 128):
             columns = slice(start, min(start + 128, UNITS))
             gate = smooth(gx, 0, columns)
             value = smooth(vx, 1, columns)
             hid[rows, columns] = (gate / (1.0 + jnp.exp(-gate)) * value).astype(BF16)
+
+    def inner_step(index, carry):
+        conv_step(index, index - 1)
         return carry
 
-    lax.fori_loop(0, 5, conv_step, 0)
-
-    weights_at("conv")
-    def down(feature):
+    lax.fori_loop(1, 4, inner_step, 0)
+
+    def down(feature, rows):
         weights = jnp.concatenate([dnf[2 * feature], dnf[2 * feature + 1]], axis=1)
-        return jnp.dot(hid[...], weights, preferred_element_type=F32)
-
-    def down_pair(dx):
-        send_a[dx] = down(place.feature(dx, 1)).astype(BF16)
-        copies.start(lambda: (send_a.at[dx], recv_a.at[dx], rs.at[dx], rr.at[dx], place.peer(0, 1)))
-        part[dx] = down(place.feature(dx))
-
-    def pair_sum(dx):
-        copies.arrived(recv_a.at[dx], rr.at[dx], place.peer(0, 1))
-        return part[dx] + recv_a[dx].astype(F32)
-
-    def send_half(side, index, dx):
-        rows = pl.ds(320 * (index % 2), 320)
-        copies.start(
-            lambda: (send_c.at[side, rows], recv_c.at[side, rows], rs.at[6 + index], rr.at[6 + index], place.peer(dx))
-        )
-
-    down_pair(2)
-    down_pair(1)
-    far = pair_sum(2)
-    send_b[0] = far[0:320].astype(BF16)
-    copies.start(lambda: (send_b.at[0], recv_b.at[0], rs.at[4], rr.at[4], place.peer(1)))
-    send_b[1] = far[320:640].astype(BF16)
-    copies.start(lambda: (send_b.at[1], recv_b.at[1], rs.at[5], rr.at[5], place.peer(3)))
-    down_pair(3)
-    right = pair_sum(1)
-    send_c[0, 320:640] = right[320:640].astype(BF16)
-    send_half(0, 1, 1)
-    part[1, 0:320] = right[0:320]
-    down_pair(0)
-    left = pair_sum(3)
-    send_c[1, 0:320] = left[0:320].astype(BF16)
-    send_half(1, 2, 3)
-    copies.arrived(recv_b.at[0], rr.at[4], place.peer(1))
-    send_c[0, 0:320] = (part[1, 0:320] + recv_b[0].astype(F32)).astype(BF16)
-    send_half(0, 0, 1)
-    copies.arrived(recv_b.at[1], rr.at[5], place.peer(3))
-    send_c[1, 320:640] = (left[320:640] + recv_b[1].astype(F32)).astype(BF16)
-    send_half(1, 3, 3)
-    own_sum = pair_sum(0) + att[tp].astype(F32)
-    for side, index in ((0, 1), (1, 2), (0, 0), (1, 3)):
-        copies.arrived(recv_c.at[side, pl.ds(320 * (index % 2), 320)], rr.at[6 + index], place.peer(1))
-    out_ref[...] = (own_sum + recv_c[0].astype(F32) + recv_c[1].astype(F32)).astype(BF16)
+        return jnp.dot(hid[rows, :], weights, preferred_element_type=F32)
+
+    class Reduce:
+        def __init__(self, start, count, first):
+            self.rows = slice(start, start + count)
+            self.halves = (slice(start, start + count // 2), slice(start + count // 2, start + count))
+            self.first = first
+
+        def move(self, ref, other, index, device):
+            index += self.first
+            copies.start(lambda: (ref(), other(), rs.at[index], rr.at[index], device()))
+
+        def landed(self, ref, index):
+            copies.arrived(ref, rr.at[index + self.first], place.peer(1))
+
+        def down_pair(self, dx):
+            rows = self.rows
+            send_a[dx, rows] = down(place.feature(dx, 1), rows).astype(BF16)
+            self.move(lambda: send_a.at[dx, rows], lambda: recv_a.at[dx, rows], dx, lambda: place.peer(0, 1))
+            part[dx, rows] = down(place.feature(dx), rows)
+
+        def pair_sum(self, dx):
+            self.landed(recv_a.at[dx, self.rows], dx)
+            return part[dx, self.rows] + recv_a[dx, self.rows].astype(F32)
+
+        def far(self):
+            total = self.pair_sum(2).astype(BF16)
+            for side, rows in enumerate(self.halves):
+                send_b[rows] = total[rows.start - self.rows.start : rows.stop - self.rows.start]
+                self.move(
+                    lambda rows=rows: send_b.at[rows], lambda rows=rows: recv_b.at[rows], 4 + side,
+                    lambda side=side: place.peer((1, 3)[side]),
+                )
+
+        def near(self, side):
+            total = self.pair_sum((1, 3)[side])
+            part[(1, 3)[side], self.rows] = total
+            rows = self.halves[1 - side]
+            send_c[side, rows] = total[rows.start - self.rows.start : rows.stop - self.rows.start].astype(BF16)
+            self.send(side, rows, 6 + side)
+
+        def send(self, side, rows, index):
+            self.move(
+                lambda: send_c.at[side, rows], lambda: recv_c.at[side, rows], index, lambda: place.peer((1, 3)[side])
+            )
+
+        def join(self):
+            for side, rows in enumerate(self.halves):
+                self.landed(recv_b.at[rows], 4 + side)
+                send_c[side, rows] = (part[(1, 3)[side], rows] + recv_b[rows].astype(F32)).astype(BF16)
+                self.send(side, rows, 8 + side)
+
+        def result(self):
+            total = self.pair_sum(0)
+            for side in range(2):
+                self.landed(recv_c.at[side, self.halves[1 - side]], 6 + side)
+                self.landed(recv_c.at[side, self.halves[side]], 8 + side)
+            return total + recv_c[0, self.rows].astype(F32) + recv_c[1, self.rows].astype(F32)
+
+    first, second = Reduce(0, 384, 0), Reduce(384, 256, 10)
+    first.down_pair(2)
+    first.down_pair(1)
+    first.far()
+    first.down_pair(3)
+    first.near(0)
+    first.down_pair(0)
+    first.near(1)
+    for rows, landing, index, device in edges:
+        copies.arrived(edge(rows, landing, index, device)[1], er.at[index], device)
+    conv_step(0, 3)
+    conv_step(4, 4)
+    second.down_pair(2)
+    second.down_pair(1)
+    second.far()
+    second.down_pair(3)
+    second.near(0)
+    first.join()
+    second.down_pair(0)
+    second.near(1)
+    second.join()
+    out_ref[128:512, :] = (att[tp, 128:512].astype(F32) + first.result()).astype(BF16)
+    rest = second.result()
+    out_ref[0:128, :] = (att[tp, 0:128].astype(F32) + rest[0:128]).astype(BF16)
+    out_ref[512:640, :] = (att[tp, 512:640].astype(F32) + rest[128:256]).astype(BF16)
     copies.drain()
 
 
@@ -709,8 +752,8 @@
             pltpu.VMEM((4, ROWS, FEATS), F32),
             pltpu.VMEM((4, ROWS, FEATS), BF16),
             pltpu.VMEM((4, ROWS, FEATS), BF16),
-            pltpu.VMEM((2, ROWS // 2, FEATS), BF16),
-            pltpu.VMEM((2, ROWS // 2, FEATS), BF16),
+            pltpu.VMEM((ROWS, FEATS), BF16),
+            pltpu.VMEM((ROWS, FEATS), BF16),
             pltpu.VMEM((2, ROWS, FEATS), BF16),
             pltpu.VMEM((2, ROWS, FEATS), BF16),
             pltpu.VMEM((NOPE_W + ROPE, ROWS), BF16),
@@ -732,7 +775,7 @@
             dma((1, 10)), dma((1, 10)),
             dma((3, 8)), dma((3, 8)),
             dma((4,)), dma((4,)),
-            dma((10,)), dma((10,)),
+            dma((20,)), dma((20,)),
             dma((16,)),
         ],
         compiler_params=pltpu.CompilerParams(

time: 121 us -> 111 us (0.917)
  Pallas kernels: 118 us -> 108 us
    pallas_call x1, Pallas kernels: 118 us -> 108 us  [per_device(): pl.pallas_call(kernel, out_shape=jax.ShapeDtypeStruct((ROWS, FEATS), BF16...]
where the time goes in v4:
time: 111 us
  Pallas kernels  108 us (97%)
  local copies, waits for them, and re-layouts  3.05 us (3%)
    pallas_call x1, Pallas kernels, per_device(): pl.pallas_call(kernel, out_shape=jax.ShapeDtypeStruct((ROWS, FEATS), BF16...  108 us
    unnamed x3, local copies, waits for them, and re-layouts  2.37 us

profile of v4, /device:TPU:1, one launch (start us, length us, event | category | flops | bytes accessed | tf_op | source)
XLA Modules:
  0.0 110.7 jit_solution(10911022755127429168)
XLA Ops:
  0.0 0.0 copy-start
  0.0 0.7 copy-done
  0.7 0.7 jit_solution_.3.inv_hbm
  1.3 107.7 %shard_map.154 = bf16[640,256]{1,0:T(8,128)(2,1)} custom-call(bf16[192,640]{1,0:T(8,128)(2,1)} %bitcast.7, bf16[640,128]{1,0:T(8,128)(2,1)} %qn_hbm.1, bf16[640,512]{1,0:T(8,128)(2,1)} %lat_hbm.1, bf16[64,640]{1,0:T(8,128)(2,1)} %bitcast.11, f32[1,512]{1,0:T(1,128)} %bitcast.12, bf16[512,256]{1,0:T(8,128)(2,1)} %ew_hbm.1, bf16[512,128]{1,0:T(8,128)(2,1)} %en_hbm.1, ...), custom_call_target="tpu_custom_call" | custom-call | tf_op jit(solution)/shard_map/pallas_call | solution.py:724
  109.0 1.7 %copy.18 = bf16[640,256]{1,0:T(8,128)(2,1)} copy(bf16[640,256]{1,0:T(8,128)(2,1)} %shard_map.154) | data formatting | bytes 655360
Async XLA Ops:
  0.0 0.7 copy-start

commit v5 on v4

--- a/solution.py
+++ b/solution.py
@@ -272,7 +272,7 @@
         mean = jnp.sum(floats * floats, axis=1, keepdims=True) * (1.0 / RANK)
         latb[half, 0] = (floats * lax.rsqrt(mean + epsilon) * lgain[...]).astype(BF16)
     position = (lax.broadcasted_iota(jnp.int32, (32, ROWS), 1) + sp * ROWS).astype(F32)
-    angles = position * inv_ref[:, 0:1]
+    angles = position * inv_ref[...]
     cosine, sine = jnp.cos(angles), jnp.sin(angles)
 
     def turn(floats):
@@ -717,7 +717,7 @@
     out_wide, out_narrow, norm_gain, up_gate, up_value, down_weight, conv_taps,
 ):
     inverse = np.power(np.float32(theta), -2.0 * np.arange(32, dtype=np.float32) / ROPE).astype(np.float32)
-    inverse = jnp.asarray(np.broadcast_to(inverse[:, None], (32, 128)))
+    inverse = jnp.asarray(inverse[:, None])
     vmem = pl.BlockSpec(memory_space=pltpu.VMEM)
     anywhere = pl.BlockSpec(memory_space=pl.ANY)
     dma = pltpu.SemaphoreType.DMA
@@ -767,7 +767,7 @@
             pltpu.VMEM((RANK, 128), BF16),
             pltpu.VMEM((ROWS, FEATS), BF16),
             pltpu.VMEM((3, 2, UNITS), F32),
-            pltpu.VMEM((32, 128), F32),
+            pltpu.VMEM((32, 1), F32),
             dma((2, N_SEND)), dma((2, 32)), dma((2, 16)), dma((2, 16)), dma((2, 16)), dma((2, 16)),
             dma((1, N_SEND)), dma((1, 32)),
             dma((1, N_SEND)), dma((1, 32)),

time: 111 us -> 110 us (level)
  local copies, waits for them, and re-layouts: 3.05 us -> 1.72 us
    unnamed x3 -> x1, local copies, waits for them, and re-layouts: 2.37 us -> 1.72 us
where the time goes in v5:
time: 110 us; the launch traced here: 109 us
  Pallas kernels  108 us (98%)
  local copies, waits for them, and re-layouts  1.72 us (2%)
    pallas_call x1, Pallas kernels, per_device(): pl.pallas_call(kernel, out_shape=jax.ShapeDtypeStruct((ROWS, FEATS), BF16...  108 us

profile of v5, /device:TPU:1, one launch (start us, length us, event | category | flops | bytes accessed | tf_op | source)
XLA Modules:
  0.0 109.5 jit_solution(15454687411861200201)
XLA Ops:
  0.0 107.8 %shard_map.154 = bf16[640,256]{1,0:T(8,128)(2,1)} custom-call(bf16[192,640]{1,0:T(8,128)(2,1)} %bitcast.7, bf16[640,128]{1,0:T(8,128)(2,1)} %qn_hbm.1, bf16[640,512]{1,0:T(8,128)(2,1)} %lat_hbm.1, bf16[64,640]{1,0:T(8,128)(2,1)} %bitcast.11, f32[1,512]{1,0:T(1,128)} %bitcast.12, bf16[512,256]{1,0:T(8,128)(2,1)} %ew_hbm.1, bf16[512,128]{1,0:T(8,128)(2,1)} %en_hbm.1, ...), custom_call_target="tpu_custom_call" | custom-call | tf_op jit(solution)/shard_map/pallas_call | solution.py:724
  107.8 1.7 %copy.18 = bf16[640,256]{1,0:T(8,128)(2,1)} copy(bf16[640,256]{1,0:T(8,128)(2,1)} %shard_map.154) | data formatting | bytes 655360
